TPU v7x, 32 devices: a whole 2x2x4 slice. The times are simulated.
32 devices in a mesh: sp: 8 (over z, x), tp: 4 (over y, core).
Axes of the slice: x: 2, y: 2, z: 4, core: 2. Of those that a mesh axis runs over, the one named last changes fastest.
Arguments:
- cot_out: bfloat16 [2048, 2048], P('sp', 'tp'), may hold values from -6 to 6
- route_ids: int32 [2048, 2], P('sp'), may hold values from 0 to 7, all different within a row; in each aligned block of 256 rows (0 to 255, 256 to 511, ...) at most 96 rows name the same one
- route_weight: float32 [2048, 2], P('sp'), may hold values from 0.1 to 1
- expert_inputs: bfloat16 [8, 768, 2048], P('sp'), may hold values from -48 to 48
- w_gate: bfloat16 [8, 2048, 1024], P('sp', None, 'tp'), may hold values from -0.125 to 0.125
- w_up: bfloat16 [8, 2048, 1024], P('sp', None, 'tp'), may hold values from -0.125 to 0.125
- w_down: bfloat16 [8, 1024, 2048], P('sp', 'tp'), may hold values from -0.1875 to 0.1875
- w_proj: bfloat16 [2048, 2048], P('tp'), may hold values from -0.125 to 0.125
- conv_out: bfloat16 [2048, 2048], P('sp', 'tp'), may hold values from -6 to 6
- channel_norm_gain: float32 [2048], P('tp'), may hold values from 0.1 to 1.9
- taps: float32 [31, 2048], P(None, 'tp'), may hold values from -1 to 1
- value_pre: bfloat16 [2048, 2048], P('sp', 'tp'), may hold values from -6 to 6
- gate_pre: bfloat16 [2048, 2048], P('sp', 'tp'), may hold values from -6 to 6
Outputs:
- grad_gate_w: bfloat16 [8, 2048, 1024], P('sp', None, 'tp')
- grad_up_w: bfloat16 [8, 2048, 1024], P('sp', None, 'tp')
- grad_down_w: bfloat16 [8, 1024, 2048], P('sp', 'tp')
- grad_proj: float32 [2048, 2048], P(('tp', 'sp'))
- grad_value: bfloat16 [2048, 2048], P('sp', 'tp')
- grad_gate: bfloat16 [2048, 2048], P('sp', 'tp')
Inputs may be any that keep to these rules, and one draw needn't show every extreme that they name: `route_ids`: among the tokens of one index of sp no expert is chosen more than 96 times, a bound that some block reaches; a token's experts differ.
All inputs are finite; a program needn't handle non-finite values.
Results may differ from a plain program's by a relative error of at most 0.012.
Values may be sent and summed in bfloat16 or wider, within the bound.
A program may use at most 128 MiB of HBM per device.

v0:
```python
import functools

import jax
import jax.numpy as jnp
from jax import lax
from jax.experimental import pallas as pl
from jax.experimental.pallas import tpu as pltpu
from jax.sharding import PartitionSpec as P

clamp_limit = 7.0
swish_alpha = 1.702
norm_epsilon = 1e-05
MESH = pl.DeviceIdType.MESH
VMEM = pltpu.VMEM


def lanes(index, width):
    return pl.ds(pl.multiple_of(index * width, width), width)


def places(group, narrow):
    me, t = lax.axis_index("sp"), lax.axis_index("tp")
    near = t + 1 - 2 * lax.rem(t, 2)
    far = lax.rem(t + narrow // 2, narrow)
    return me, t, near, far, lax.rem(near + narrow // 2, narrow)


def spread(pairs):
    return sorted(range(1, pairs), key=lambda o: abs(2 * o - pairs))


def around(me, group, sign):
    pairs = group // 2
    half, parity = me // 2, lax.rem(me, 2)
    across = [
        2 * lax.rem(half + pairs + sign * o, pairs) + (parity if side == 0 else 1 - parity)
        for o in spread(pairs)
        for side in range(2)
    ]
    return 2 * half + 1 - parity, across


def remote(src, dst, send, recv, sp, tp):
    return pltpu.make_async_remote_copy(
        src_ref=src, dst_ref=dst, send_sem=send, recv_sem=recv, device_id=(sp, tp), device_id_type=MESH
    )


def meet(peers):
    barrier = pltpu.get_barrier_semaphore()
    for sp, tp in peers:
        pl.semaphore_signal(barrier, inc=1, device_id=(sp, tp), device_id_type=MESH)
    pl.semaphore_wait(barrier, len(peers))


def dispatch_kernel(
    group,
    narrow,
    width,
    out_ref,
    stat_ref,
    in_ref,
    gate_ref,
    up_ref,
    rows_ref,
    stats_ref,
    gate_lin_ref,
    up_lin_ref,
    *sems,
):
    a_s, a_r, n_s, n_r, f_s, f_r, m_s, m_r, t_s, t_r, l_s = sems
    me, t, near, far, cross = places(group, narrow)
    partner, across = around(me, group, 1)
    sp_peers = [partner] + across
    meet([(p, t) for p in sp_peers] + [(me, near), (me, far), (me, cross)])

    def spot(s, column):
        return rows_ref.at[s, :, lanes(column, width)]

    def swap(s):
        return remote(out_ref.at[s], spot(me, t), a_s.at[s], a_r.at[me], s, t)

    for p in sp_peers:
        swap(p).start()
    stat_own = pltpu.make_async_copy(stat_ref, stats_ref.at[t], l_s.at[0])
    stat_own.start()
    small = []
    for k, p in enumerate((near, far, cross)):
        c = remote(stat_ref, stats_ref.at[t], t_s.at[k], t_r.at[k], me, p)
        c.start()
        small.append(c)
    own = pltpu.make_async_copy(out_ref.at[me], spot(me, t), l_s.at[1])
    own.start()
    own.wait()
    order = [me, partner] + around(me, group, -1)[1]

    def to_far(s):
        return remote(spot(s, t), spot(s, t), f_s.at[s], f_r.at[s], me, far)

    def to_near(s):
        return remote(spot(s, t), spot(s, t), n_s.at[s], n_r.at[s], me, near)

    def onward(s):
        return remote(spot(s, far), spot(s, far), m_s.at[s], m_r.at[s], me, near)

    def relay(s):
        to_far(s).wait_recv()
        onward(s).start()

    turns = 8
    count = in_ref.shape[0] // turns

    def multiply(piece):
        span = pl.ds(piece * count, count)
        rows = in_ref[span, :]
        gate_lin_ref[span, :] = jnp.dot(rows, gate_ref[...], preferred_element_type=jnp.float32)
        up_lin_ref[span, :] = jnp.dot(rows, up_ref[...], preferred_element_type=jnp.float32)

    lag = min(2, group)
    for i, s in enumerate(order):
        if i > 0:
            remote(out_ref.at[s], spot(s, t), a_s.at[s], a_r.at[s], s, t).wait_recv()
        to_far(s).start()
        to_near(s).start()
        if i >= lag:
            relay(order[i - lag])
        for piece in range(turns * i // group, turns * (i + 1) // group):
            multiply(piece)
    for s in order[group - lag :]:
        relay(s)
    for s in order:
        to_far(s).wait_send()
        to_near(s).wait_send()
        onward(s).wait_send()
        remote(spot(s, near), spot(s, near), n_s.at[s], n_r.at[s], me, near).wait_recv()
        remote(spot(s, cross), spot(s, cross), m_s.at[s], m_r.at[s], me, near).wait_recv()
    for p in sp_peers:
        swap(p).wait_send()
    stat_own.wait()
    for c in small:
        c.wait_send()
        c.wait_recv()


def dispatch(outgoing, stat, rows_in, gate_weight, up_weight):
    group, capacity, width = outgoing.shape
    narrow = lax.axis_size("tp")
    dma = pltpu.SemaphoreType.DMA
    return pl.pallas_call(
        functools.partial(dispatch_kernel, group, narrow, width),
        out_shape=(
            jax.ShapeDtypeStruct((group, capacity, narrow * width), outgoing.dtype),
            jax.ShapeDtypeStruct((narrow,) + stat.shape, stat.dtype),
            jax.ShapeDtypeStruct((rows_in.shape[0], gate_weight.shape[1]), jnp.float32),
            jax.ShapeDtypeStruct((rows_in.shape[0], up_weight.shape[1]), jnp.float32),
        ),
        in_specs=[pl.BlockSpec(memory_space=VMEM)] * 5,
        out_specs=[pl.BlockSpec(memory_space=VMEM)] * 4,
        scratch_shapes=[dma((group,))] * 8 + [dma((3,))] * 2 + [dma((2,))],
        compiler_params=pltpu.CompilerParams(collective_id=0, has_side_effects=True),
    )(outgoing, stat, rows_in, gate_weight, up_weight)


def return_kernel(group, narrow, width, part_ref, home_ref, pair_buf, far_out, far_in, done, *sems):
    n_s, n_r, f_s, f_r, a_s, a_r, l_s = sems
    me, t, near, far, cross = places(group, narrow)
    partner, across = around(me, group, 1)
    sp_peers = across + [partner]
    meet([(p, t) for p in sp_peers] + [(me, near), (me, far)])
    order = sp_peers + [me]

    def part(s, column):
        return part_ref.at[s, :, lanes(column, width)]

    def to_near(s, k):
        return remote(
            part(s, near if k == 0 else cross), pair_buf.at[s, k], n_s.at[s, k], n_r.at[s, k], me, near
        )

    def to_far(s):
        return remote(far_out.at[s], far_in.at[s], f_s.at[s], f_r.at[s], me, far)

    def to_home(s):
        return remote(done.at[s], home_ref.at[me], a_s.at[s], a_r.at[me], s, t)

    for s in order:
        to_near(s, 1).start()
    for s in order:
        to_near(s, 0).start()
    own = pltpu.make_async_copy(done.at[me], home_ref.at[me], l_s.at[0])

    def finish(s, i):
        to_near(s, 0).wait_recv()
        to_far(s).wait_recv()
        total = part_ref[s, :, lanes(t, width)].astype(jnp.float32)
        total = total + pair_buf[s, 0].astype(jnp.float32) + far_in[s].astype(jnp.float32)
        done[s] = total.astype(done.dtype)
        if i < group - 1:
            to_home(s).start()
        else:
            own.start()

    for s in order:
        to_near(s, 1).wait_recv()
        pair = part_ref[s, :, lanes(far, width)].astype(jnp.float32) + pair_buf[s, 1].astype(jnp.float32)
        far_out[s] = pair.astype(far_out.dtype)
        to_far(s).start()
    for i, s in enumerate(order):
        finish(s, i)
    own.wait()
    for s in order:
        to_near(s, 0).wait_send()
        to_near(s, 1).wait_send()
        to_far(s).wait_send()
    for s in sp_peers:
        to_home(s).wait_send()
        remote(done.at[s], home_ref.at[s], a_s.at[s], a_r.at[s], s, t).wait_recv()


def return_home(partial):
    group, capacity, whole = partial.shape
    narrow = lax.axis_size("tp")
    width = whole // narrow
    dma = pltpu.SemaphoreType.DMA
    block = (group, capacity, width)
    return pl.pallas_call(
        functools.partial(return_kernel, group, narrow, width),
        out_shape=jax.ShapeDtypeStruct(block, partial.dtype),
        in_specs=[pl.BlockSpec(memory_space=VMEM)],
        out_specs=pl.BlockSpec(memory_space=VMEM),
        scratch_shapes=[
            VMEM((group, 2, capacity, width), partial.dtype),
            VMEM(block, partial.dtype),
            VMEM(block, partial.dtype),
            VMEM(block, partial.dtype),
        ]
        + [dma((group, 2))] * 2
        + [dma((group,))] * 4
        + [dma((1,))],
        compiler_params=pltpu.CompilerParams(collective_id=1, has_side_effects=True),
    )(partial)


def widen_kernel(narrow, width, pieces, mix_ref, full_ref, *sems):
    n_s, n_r, f_s, f_r, m_s, m_r, l_s = sems
    me, t, near, far, cross = places(1, narrow)
    meet([(me, near), (me, far)])
    rows = mix_ref.shape[0] // pieces

    def src(k):
        return mix_ref.at[pl.ds(k * rows, rows)]

    def spot(k, column):
        return full_ref.at[pl.ds(k * rows, rows), lanes(column, width)]

    def to_far(k):
        return remote(src(k), spot(k, t), f_s.at[k], f_r.at[k], me, far)

    def to_near(k):
        return remote(src(k), spot(k, t), n_s.at[k], n_r.at[k], me, near)

    def onward(k):
        return remote(spot(k, far), spot(k, far), m_s.at[k], m_r.at[k], me, near)

    own = pltpu.make_async_copy(mix_ref, full_ref.at[:, lanes(t, width)], l_s.at[0])
    for k in range(pieces):
        to_far(k).start()
    for k in range(pieces):
        to_near(k).start()
    own.start()
    for k in range(pieces):
        to_far(k).wait_recv()
        onward(k).start()
    own.wait()
    for k in range(pieces):
        to_far(k).wait_send()
        to_near(k).wait()
        onward(k).wait()


def widen(mix):
    rows, width = mix.shape
    narrow = lax.axis_size("tp")
    pieces = 4
    dma = pltpu.SemaphoreType.DMA
    return pl.pallas_call(
        functools.partial(widen_kernel, narrow, width, pieces),
        out_shape=jax.ShapeDtypeStruct((rows, narrow * width), mix.dtype),
        in_specs=[pl.BlockSpec(memory_space=VMEM)],
        out_specs=pl.BlockSpec(memory_space=VMEM),
        scratch_shapes=[dma((pieces,))] * 6 + [dma((1,))],
        compiler_params=pltpu.CompilerParams(collective_id=2, has_side_effects=True),
    )(mix)


def tail_kernel(
    group,
    narrow,
    reach,
    parts_ref,
    grad_ref,
    hat_ref,
    stat_ref,
    taps_ref,
    proj_ref,
    others,
    glu_ref,
    stats,
    next_stats,
    next_grad,
    next_hat,
    extended,
    pair_in,
    pair_sum,
    *sems,
):
    t_s, t_r, v_s, v_r, h_s, h_r, x_s, x_r, z_s, z_r = sems
    f32 = jnp.float32
    me, t, near, far, cross = places(group, narrow)
    rows, cols = grad_ref.shape
    halo = next_grad.shape[0]
    pairs = group // 2
    parity = lax.rem(me, 2)
    half = me // 2
    partner = me + 1 - 2 * parity
    ahead, behind = lax.rem(me + 1, group), lax.rem(me + group - 1, group)
    siblings = [lax.rem(t + o, narrow) for o in range(1, narrow)]
    alike = [lax.rem(half + o, pairs) for o in spread(pairs)]
    cut = parts_ref.shape[2] // 2
    sides = [pl.ds(h * cut, cut) for h in range(2)]
    everyone = [t] + siblings
    meet(
        [(me, p) for p in siblings]
        + [(ahead, p) for p in everyone]
        + [(behind, p) for p in everyone]
        + [(partner, t)]
        + [(2 * q + parity, t) for q in alike]
    )
    sends = []
    for k, p in enumerate(siblings):
        sends.append(remote(stat_ref, stats.at[k], t_s.at[k], t_r.at[k], me, p))
    for k, p in enumerate(everyone):
        sends.append(remote(stat_ref, next_stats.at[k], v_s.at[k], v_r.at[k], behind, p))
    sends.append(remote(grad_ref.at[pl.ds(0, halo)], next_grad, h_s.at[0], h_r.at[0], behind, t))
    sends.append(remote(hat_ref.at[pl.ds(0, halo)], next_hat, h_s.at[1], h_r.at[1], behind, t))
    for c in sends:
        c.start()

    def swap(q, h):
        side = sides[h]
        return remote(
            parts_ref.at[2 * q + 1 - parity, :, side],
            pair_in.at[q, :, side],
            x_s.at[q, h],
            x_r.at[q, h],
            partner,
            t,
        )

    def passing(source, target, h):
        slot = others.at[slot_of(source, target), :, sides[h]]
        return slot, z_r.at[source, h]

    def scatter(q, h):
        slot, arrival = passing(half, q, h)
        return remote(pair_sum.at[q, :, sides[h]], slot, z_s.at[q, h], arrival, 2 * q + parity, t)

    def slot_of(source, target):
        return lax.rem(target - source + pairs, pairs) - 1

    order = alike + [half]
    for q in order:
        for h in range(2):
            swap(q, h).start()
    for c in sends:
        c.wait_recv()

    channels = cols * narrow

    def finished(grad, hat, total, own):
        total = jnp.transpose(total)
        deviation = jnp.transpose(own)[:, 2:3]
        count = grad.shape[0]
        first, second = total[:count, 0:1] / channels, total[:count, 1:2] / channels
        return deviation[:count] * (grad - first - hat * second)

    total = stat_ref[...]
    following = next_stats[0]
    for k in range(narrow - 1):
        total = total + stats[k]
        following = following + next_stats[k + 1]
    extended[pl.ds(0, rows), :] = finished(grad_ref[...], hat_ref[...], total, stat_ref[...])
    beyond = finished(next_grad[...], next_hat[...], following, next_stats[0])
    extended[pl.ds(rows, halo), :] = jnp.where(me == group - 1, jnp.zeros_like(beyond), beyond)

    step = 32
    strips = cols // 128

    def convolve(index, carry):
        start = pl.multiple_of((index // strips) * step, step)
        column = lanes(lax.rem(index, strips), 128)
        total = jnp.zeros((step, 128), f32)
        window = extended[pl.ds(start, step + halo), column]
        for turn in range(8):
            shifted = window if turn == 0 else pltpu.roll(window, step + halo - turn, 0)
            for j in range(turn, reach, 8):
                total = total + taps_ref[reach - 1 - j : reach - j, column] * shifted[j - turn : j - turn + step]
        glu_ref[pl.ds(start, step), column] = total
        return carry

    turns = rows // step * strips
    marks = [turns * i // (2 * pairs) for i in range(2 * pairs + 1)]
    for i, q in enumerate(order):
        for h in range(2):
            lax.fori_loop(marks[2 * i + h], marks[2 * i + h + 1], convolve, 0)
            swap(q, h).wait_recv()
            both = parts_ref[2 * q + parity, :, sides[h]].astype(f32) + pair_in[q, :, sides[h]].astype(f32)
            if i < pairs - 1:
                pair_sum[q, :, sides[h]] = both.astype(pair_sum.dtype)
                scatter(q, h).start()
            else:
                proj_ref[:, sides[h]] = both
    for q in alike:
        for h in range(2):
            slot, arrival = passing(q, half, h)
            remote(pair_sum.at[q, :, sides[h]], slot, z_s.at[q, h], arrival, 2 * q + parity, t).wait_recv()
    for c in sends:
        c.wait_send()
    for h in range(2):
        for q in order:
            swap(q, h).wait_send()
        for q in alike:
            scatter(q, h).wait_send()


def tail(parts, grad, hat, stat, taps):
    group, block, model = parts.shape
    rows, cols = grad.shape
    narrow = lax.axis_size("tp")
    reach = taps.shape[0]
    halo = -(-(reach - 1) // 8) * 8
    pairs = group // 2
    f32 = jnp.float32
    dma = pltpu.SemaphoreType.DMA
    return pl.pallas_call(
        functools.partial(tail_kernel, group, narrow, reach),
        out_shape=(
            jax.ShapeDtypeStruct((block, model), f32),
            jax.ShapeDtypeStruct((pairs - 1, block, model), parts.dtype),
            jax.ShapeDtypeStruct((rows, cols), f32),
        ),
        in_specs=[pl.BlockSpec(memory_space=VMEM)] * 5,
        out_specs=[pl.BlockSpec(memory_space=VMEM)] * 3,
        scratch_shapes=[
            VMEM((narrow - 1,) + stat.shape, f32),
            VMEM((narrow,) + stat.shape, f32),
            VMEM((halo, cols), f32),
            VMEM((halo, cols), f32),
            VMEM((rows + halo, cols), f32),
            VMEM((pairs, block, model), parts.dtype),
            VMEM((pairs, block, model), parts.dtype),
            dma((narrow - 1,)),
            dma((narrow - 1,)),
            dma((narrow,)),
            dma((narrow,)),
            dma((2,)),
            dma((2,)),
        ]
        + [dma((pairs, 2))] * 4,
        compiler_params=pltpu.CompilerParams(collective_id=3, has_side_effects=True),
    )(parts, grad, hat, stat, taps)


def per_device(
    cot_out,
    route_ids,
    route_weight,
    expert_inputs,
    w_gate,
    w_up,
    w_down,
    w_proj,
    conv_out,
    channel_norm_gain,
    taps,
    value_pre,
    gate_pre,
):
    group_size = lax.axis_size("sp")
    narrow_size = lax.axis_size("tp")
    tok_rows, local_cols = cot_out.shape
    chosen = route_ids.shape[1]
    slot_rows = expert_inputs.shape[1]
    capacity = slot_rows // group_size
    model_width = expert_inputs.shape[2]
    f32, bf16 = jnp.float32, jnp.bfloat16
    experts = jnp.arange(group_size, dtype=jnp.int32)[None, :]
    hots = [(route_ids[:, k : k + 1] == experts) for k in range(chosen)]
    hot = functools.reduce(jnp.logical_or, hots)
    token = jnp.arange(tok_rows, dtype=jnp.int32)
    before = (token[:, None] > token[None, :]).astype(bf16)
    earlier = jnp.dot(before, hot.astype(bf16), preferred_element_type=f32)
    slots = jnp.arange(slot_rows, dtype=jnp.int32)[None, :]
    picks, scaled = [], []
    for k in range(chosen):
        slot = jnp.sum(jnp.where(hots[k], earlier, 0.0), axis=1).astype(jnp.int32)
        dest = route_ids[:, k] * capacity + slot
        picks.append((dest[:, None] == slots).astype(bf16))
        scaled.append((route_weight[:, k : k + 1] * cot_out.astype(f32)).astype(bf16))
    outgoing = lax.dot_general(
        jnp.concatenate(picks, axis=0),
        jnp.concatenate(scaled, axis=0),
        (((0,), (0,)), ((), ())),
        preferred_element_type=f32,
    ).astype(bf16)
    convolution_filter = conv_out.astype(f32)
    stat = jnp.stack(
        [jnp.sum(convolution_filter, axis=1), jnp.sum(convolution_filter * convolution_filter, axis=1)]
    )
    rows_in = expert_inputs[0]
    gate_weight = w_gate[0]
    up_weight = w_up[0]
    down_weight = w_down[0]
    arrived, stats, gate_lin, up_lin = dispatch(
        outgoing.reshape(group_size, capacity, local_cols), stat, rows_in, gate_weight, up_weight
    )
    rows_cot = arrived.reshape(slot_rows, model_width)
    gate_c = jnp.minimum(gate_lin, clamp_limit)
    up_c = jnp.clip(up_lin, -clamp_limit, clamp_limit)
    sigma = jax.nn.sigmoid(swish_alpha * gate_c)
    act = ((up_c + 1.0) * gate_c * sigma).astype(bf16)
    grad_down = jnp.dot(act.T, rows_cot, preferred_element_type=f32).astype(bf16)
    d_act = jnp.dot(rows_cot, down_weight.T, preferred_element_type=f32)
    up_open = ((up_lin > -clamp_limit) & (up_lin < clamp_limit)).astype(f32)
    gate_open = (gate_lin < clamp_limit).astype(f32)
    d_up = (d_act * gate_c * sigma * up_open).astype(bf16)
    d_gate = (
        d_act * (up_c + 1.0) * (sigma + swish_alpha * gate_c * sigma * (1.0 - sigma)) * gate_open
    ).astype(bf16)
    grad_gate_part = jnp.dot(rows_in.T, d_gate, preferred_element_type=f32).astype(bf16)
    grad_up_part = jnp.dot(rows_in.T, d_up, preferred_element_type=f32).astype(bf16)
    partial_value = jnp.dot(d_gate, gate_weight.T, preferred_element_type=f32)
    partial_value = partial_value + jnp.dot(d_up, up_weight.T, preferred_element_type=f32)
    coming = return_home(partial_value.astype(bf16).reshape(group_size, capacity, model_width))
    pick_any = functools.reduce(jnp.add, picks)
    summed = jnp.dot(pick_any, coming.reshape(slot_rows, local_cols), preferred_element_type=f32)
    mix_grad = (cot_out.astype(f32) + summed).astype(bf16)
    mix_full = widen(mix_grad)
    channel_total = local_cols * narrow_size
    first_sum, square_sum = jnp.sum(stats, axis=0)
    channel_mean = (first_sum / channel_total)[:, None]
    var = (square_sum / channel_total)[:, None] - channel_mean * channel_mean
    inverse_deviation = lax.rsqrt(var + norm_epsilon)
    normalized_input = (convolution_filter - channel_mean) * inverse_deviation
    normalized_output = normalized_input * channel_norm_gain[None, :]
    sigma_conv = jax.nn.sigmoid(normalized_output)
    act_conv = (normalized_output * sigma_conv).astype(bf16)
    partial_proj = lax.dot_general(
        act_conv, mix_full, (((0,), (0,)), ((), ())), preferred_element_type=f32
    ).astype(bf16)
    d_act_conv = jnp.dot(mix_full, w_proj.T, preferred_element_type=f32)
    normalized_gradient = (
        d_act_conv
        * sigma_conv
        * (1.0 + normalized_output * (1.0 - sigma_conv))
        * channel_norm_gain[None, :]
    )
    terms = jnp.stack(
        [
            jnp.sum(normalized_gradient, axis=1),
            jnp.sum(normalized_gradient * normalized_input, axis=1),
            inverse_deviation[:, 0],
        ]
    )
    terms = jnp.pad(terms, ((0, 8 - terms.shape[0]), (0, 0)))
    own_proj, other_proj, d_glu = tail(
        partial_proj.reshape(group_size, local_cols // group_size, model_width),
        normalized_gradient,
        normalized_input,
        terms,
        taps,
    )
    grad_proj = own_proj + jnp.sum(other_proj.astype(f32), axis=0)
    gate_sig = jax.nn.sigmoid(gate_pre.astype(f32))
    grad_value = (d_glu * gate_sig).astype(bf16)
    grad_gate = (d_glu * value_pre.astype(f32) * gate_sig * (1.0 - gate_sig)).astype(bf16)
    return (
        grad_gate_part[None],
        grad_up_part[None],
        grad_down[None],
        grad_proj,
        grad_value,
        grad_gate,
    )


def solution(mesh):
    return jax.shard_map(
        per_device,
        mesh=mesh,
        in_specs=(
            P("sp", "tp"),
            P("sp", None),
            P("sp", None),
            P("sp", None, None),
            P("sp", None, "tp"),
            P("sp", None, "tp"),
            P("sp", "tp", None),
            P("tp", None),
            P("sp", "tp"),
            P("tp"),
            P(None, "tp"),
            P("sp", "tp"),
            P("sp", "tp"),
        ),
        out_specs=(
            P("sp", None, "tp"),
            P("sp", None, "tp"),
            P("sp", "tp", None),
            P(("tp", "sp"), None),
            P("sp", "tp"),
            P("sp", "tp"),
        ),
        check_vma=False,
    )
```

profile of v0, /device:TPU:0, one launch (start us, length us, event | category | flops | bytes accessed | tf_op | source)
XLA Modules:
  0.0 159.3 jit_solution(995018439855645709)
XLA Ops:
  0.6 0.0 copy-start
  0.6 0.9 fusion.47
  1.5 0.8 fusion.48
  2.3 0.2 select_reduce_fusion.1
  2.5 0.8 multiply_add_fusion.1
  3.2 1.1 convert_reduce_fusion.1
  4.4 0.6 pad_maximum_fusion.stat_ref
  5.0 1.1 fusion.13
  6.1 0.2 fusion.11
  6.3 1.5 convolution_convert_fusion.4
  7.7 0.0 copy-start.14
  7.7 39.1 %shard_map.172 = (bf16[8,96,2048]{2,1,0:T(8,128)(2,1)}, f32[4,2,256]{2,1,0:T(2,128)}, f32[768,256]{1,0:T(8,128)}, f32[768,256]{1,0:T(8,128)}) custom-call(bf16[8,96,512]{2,1,0:T(8,128)(2,1)} %bitcast.60, f32[2,256]{1,0:T(2,128)} %pad_maximum_fusion.stat_ref, bf16[768,2048]{1,0:T(8,128)(2,1)} %bitcast.58, bf16[2048,256]{1,0:T(8,128)(2,1)} %bitcast.56, ...), custom_call_target="tpu_custom_call" | custom-call | tf_op jit(solution)/shard_map/pallas_call | solution.py:149
  46.9 0.7 reduce_sum.76
  47.6 0.6 add_rsqrt_fusion.1
  48.2 0.0 copy-done.14
  48.2 0.0 copy-start.13
  48.2 0.0 copy-start.15
  48.2 0.0 copy-start.16
  48.2 3.9 %select_convert_fusion = (bf16[768,256]{1,0:T(8,128)(2,1)S(1)}, bf16[768,256]{1,0:T(8,128)(2,1)S(1)}) fusion(f32[768,256]{1,0:T(8,128)} %get-tuple-element.15, f32[768,256]{1,0:T(8,128)} %get-tuple-element.13, bf16[768,2048]{1,0:T(8,128)(2,1)} %bitcast.80, bf16[1,256,2048]{2,1,0:T(8,128)(2,1)S(1)} %copy-done.14), kind=kOutput, calls=%fused_computation.21 | convolution fusion | flops 809828352 | bytes 6553600 | tf_op jit(solution)/shard_map/dot_general | solution.py:533
  52.1 0.0 copy-done.13
  52.1 0.0 copy-done.15
  52.1 0.0 copy-done.16
  52.1 0.0 copy-start.6
  52.1 0.0 copy-start.3
  52.1 2.1 %fusion.2 = bf16[1,256,2048]{2,1,0:T(8,128)(2,1)} fusion(bf16[768,2048]{1,0:T(8,128)(2,1)S(1)} %bitcast.81, f32[768,256]{1,0:T(8,128)S(1)} %copy-done.15, f32[768,256]{1,0:T(8,128)S(1)} %copy-done.16), kind=kOutput, calls=%fused_computation.7 | convolution fusion | flops 807796736 | bytes 5767168 | tf_op jit(solution)/shard_map/dot_general | solution.py:532
  54.2 0.0 copy-done.6
  54.2 0.0 copy-done.3
  54.2 1.0 fusion.1
  55.3 1.3 copy.20
  56.6 0.0 copy-start.1
  56.6 3.9 %fusion = bf16[1,2048,256]{1,2,0:T(8,128)(2,1)} fusion(bf16[768,256]{1,0:T(8,128)(2,1)S(1)} %get-tuple-element.33, bf16[1,768,2048]{2,1,0:T(8,128)(2,1)} %param.16), kind=kOutput, calls=%fused_computation.5 | convolution fusion | flops 805830656 | bytes 4587520 | tf_op jit(solution)/shard_map/dot_general | solution.py:540
  60.5 2.3 %copy.19 = bf16[1,2048,256]{2,1,0:T(8,128)(2,1)} copy(bf16[1,2048,256]{1,2,0:T(8,128)(2,1)} %fusion) | data formatting | bytes 2097152
  62.8 0.0 copy-done.1
  62.8 0.0 copy-start.2
  62.8 0.0 copy-start.7
  62.8 1.0 fusion.36
  63.8 0.2 copy-done.2
  64.0 0.1 copy-done.7
  64.1 2.7 %add_convert_fusion = bf16[768,2048]{1,0:T(8,128)(2,1)} fusion(f32[768,2048]{1,0:T(8,128)S(1)} %fusion.36, bf16[768,256]{1,0:T(8,128)(2,1)S(1)} %copy-done.7, bf16[1,2048,256]{2,1,0:T(8,128)(2,1)S(1)} %copy-done.2), kind=kOutput, calls=%fused_computation | convolution fusion | flops 808452096 | bytes 10878976 | tf_op jit(solution)/shard_map/dot_general | solution.py:543
  66.7 0.0 copy-start.8
  66.7 0.0 copy-start.9
  66.7 0.0 copy-start.12
  66.7 0.0 copy-start.17
  66.8 30.0 %shard_map.173 = bf16[8,96,512]{2,1,0:T(8,128)(2,1)} custom-call(bf16[8,96,2048]{2,1,0:T(8,128)(2,1)} %bitcast.55), custom_call_target="tpu_custom_call" | custom-call | tf_op jit(solution)/shard_map/pallas_call | solution.py:226
  96.8 0.0 copy-done.8
  96.8 2.3 %fusion.5.mix_ref = bf16[256,512]{1,0:T(8,128)(2,1)} fusion(bf16[768,512]{1,0:T(8,128)(2,1)} %bitcast.61, bf16[256,512]{1,0:T(8,128)(2,1)S(1)} %copy-done.8, s32[256]{0:T(256)S(1)} %bitcast.65, s32[256]{0:T(256)S(1)} %bitcast.63), kind=kOutput, calls=%fused_computation.14 | convolution fusion | flops 203292672 | bytes 1312768 | tf_op jit(solution)/shard_map/dot_general | solution.py:546
  99.0 11.3 %shard_map.174 = bf16[256,2048]{1,0:T(8,128)(2,1)} custom-call(bf16[256,512]{1,0:T(8,128)(2,1)} %fusion.5.mix_ref), custom_call_target="tpu_custom_call" | custom-call | tf_op jit(solution)/shard_map/pallas_call | solution.py:286
  110.3 0.0 copy-done
  110.4 0.0 copy-done.9
  110.4 0.0 copy-done.12
  110.4 0.0 copy-done.17
  110.4 0.0 copy-start.4
  110.4 3.1 %fusion.46 = (f32[256]{0:T(256)S(1)}, f32[256]{0:T(256)S(1)}, f32[256,512]{1,0:T(8,128)}, f32[256,512]{1,0:T(8,128)}) fusion(f32[256]{0:T(256)S(1)} %copy-done.12, f32[256]{0:T(256)S(1)} %bitcast.71, bf16[256,512]{1,0:T(8,128)(2,1)S(1)} %copy-done.9, f32[512]{0:T(512)S(1)} %copy-done.17, bf16[256,2048]{1,0:T(8,128)(2,1)} %shard_map.174, ...), kind=kOutput, calls=%fused_computation.84 | convolution fusion | flops 538967552 | bytes 4462592 | tf_op jit(solution)/shard_map/dot_general | solution.py:561
  113.5 0.6 select_maximum_fusion.stat_ref
  114.1 0.0 copy-done.4
  114.1 2.3 %convolution_convert_fusion = bf16[512,2048]{1,0:T(8,128)(2,1)} fusion(bf16[256,2048]{1,0:T(8,128)(2,1)S(1)} %copy-done.4, f32[512]{0:T(512)S(1)} %copy-done.17, bf16[256,512]{1,0:T(8,128)(2,1)S(1)} %copy-done.9, f32[256]{0:T(256)S(1)} %copy-done.12, f32[256]{0:T(256)S(1)} %bitcast.72), kind=kOutput, calls=%fused_computation.1 | convolution fusion | flops 539099136 | bytes 3411968 | tf_op jit(solution)/shard_map/dot_general | solution.py:558
  116.4 38.6 %shard_map.175 = (f32[64,2048]{1,0:T(8,128)}, bf16[3,64,2048]{2,1,0:T(8,128)(2,1)}, f32[256,512]{1,0:T(8,128)}) custom-call(bf16[8,64,2048]{2,1,0:T(8,128)(2,1)} %bitcast.59, f32[256,512]{1,0:T(8,128)} %get-tuple-element.48.grad_ref, f32[256,512]{1,0:T(8,128)} %get-tuple-element.36.hat_ref, f32[8,256]{1,0:T(8,128)} %select_maximum_fusion.stat_ref, ...), custom_call_target="tpu_custom_call" | custom-call | tf_op jit(solution)/shard_map/pallas_call | solution.py:445
  155.0 0.0 copy-start.5
  155.0 1.4 convert_reduce_fusion
  156.3 1.9 %add.71 = f32[64,2048]{1,0:T(8,128)} add(f32[64,2048]{1,0:T(8,128)} %get-tuple-element.17, f32[64,2048]{1,0:T(8,128)S(1)} %convert_reduce_fusion) | non-fusion elementwise | flops 131072 | bytes 1572864 | tf_op jit(solution)/shard_map/add | solution.py:583
  158.2 0.0 copy-done.10
  158.2 0.0 copy-done.11
  158.2 0.0 copy-done.5
  158.2 1.0 multiply_convert_fusion.1
  (5 shorter events, 0.0 us)
Async XLA Ops:
  0.6 109.7 %copy-start = (bf16[512,2048]{1,0:T(8,128)(2,1)S(1)}, bf16[512,2048]{1,0:T(8,128)(2,1)}, u32[]{:S(2)}) copy-start(bf16[512,2048]{1,0:T(8,128)(2,1)} %param.20) | copy-start | bytes 6291460
  7.7 40.4 %copy-start.14 = (bf16[1,256,2048]{2,1,0:T(8,128)(2,1)S(1)}, bf16[1,256,2048]{2,1,0:T(8,128)(2,1)}, u32[]{:S(2)}) copy-start(bf16[1,256,2048]{2,1,0:T(8,128)(2,1)} %param.19) | copy-start | bytes 3145732
  48.2 3.9 %copy-start.13 = (bf16[8,96,2048]{2,1,0:T(8,128)(2,1)S(1)}, bf16[8,96,2048]{2,1,0:T(8,128)(2,1)}, u32[]{:S(2)}) copy-start(bf16[8,96,2048]{2,1,0:T(8,128)(2,1)} %get-tuple-element.14) | copy-start | bytes 9437188
  48.2 3.9 %copy-start.15 = (f32[768,256]{1,0:T(8,128)S(1)}, f32[768,256]{1,0:T(8,128)}, u32[]{:S(2)}) copy-start(f32[768,256]{1,0:T(8,128)} %get-tuple-element.13) | copy-start | bytes 2359300
  48.2 3.9 %copy-start.16 = (f32[768,256]{1,0:T(8,128)S(1)}, f32[768,256]{1,0:T(8,128)}, u32[]{:S(2)}) copy-start(f32[768,256]{1,0:T(8,128)} %get-tuple-element.15) | copy-start | bytes 2359300
  52.1 2.2 %copy-start.6 = (bf16[768,256]{1,0:T(8,128)(2,1)}, bf16[768,256]{1,0:T(8,128)(2,1)S(1)}, u32[]{:S(2)}) copy-start(bf16[768,256]{1,0:T(8,128)(2,1)S(1)} %get-tuple-element.32) | copy-start | bytes 1179652
  52.1 2.2 %copy-start.3 = (bf16[1,768,2048]{2,1,0:T(8,128)(2,1)S(1)}, bf16[1,768,2048]{2,1,0:T(8,128)(2,1)}, u32[]{:S(2)}) copy-start(bf16[1,768,2048]{2,1,0:T(8,128)(2,1)} %param.16) | copy-start | bytes 9437188
  56.6 6.2 %copy-start.1 = (bf16[1,2048,256]{2,1,0:T(8,128)(2,1)S(1)}, bf16[1,2048,256]{2,1,0:T(8,128)(2,1)}, u32[]{:S(2)}) copy-start(bf16[1,2048,256]{2,1,0:T(8,128)(2,1)} %param.17) | copy-start | bytes 3145732
  62.8 1.2 copy-start.2
  62.8 1.3 copy-start.7
  66.7 30.0 %copy-start.8 = (bf16[256,512]{1,0:T(8,128)(2,1)S(1)}, bf16[256,512]{1,0:T(8,128)(2,1)}, u32[]{:S(2)}) copy-start(bf16[256,512]{1,0:T(8,128)(2,1)} %param.13) | copy-start | bytes 786436
  66.7 43.6 %copy-start.9 = (bf16[256,512]{1,0:T(8,128)(2,1)S(1)}, bf16[256,512]{1,0:T(8,128)(2,1)}, u32[]{:S(2)}) copy-start(bf16[256,512]{1,0:T(8,128)(2,1)} %param.21) | copy-start | bytes 786436
  66.7 43.6 %copy-start.12 = (f32[256]{0:T(256)S(1)}, f32[256]{0:T(256)}, u32[]{:S(2)}) copy-start(f32[256]{0:T(256)} %add_rsqrt_fusion.1) | copy-start | bytes 3076
  66.7 43.6 %copy-start.17 = (f32[512]{0:T(512)S(1)}, f32[512]{0:T(512)}, u32[]{:S(2)}) copy-start(f32[512]{0:T(512)} %param.22) | copy-start | bytes 6148
  110.4 3.7 %copy-start.4 = (bf16[256,2048]{1,0:T(8,128)(2,1)S(1)}, bf16[256,2048]{1,0:T(8,128)(2,1)}, u32[]{:S(2)}) copy-start(bf16[256,2048]{1,0:T(8,128)(2,1)} %shard_map.174) | copy-start | bytes 3145732
  116.4 41.8 %copy-start.10 = (bf16[256,512]{1,0:T(8,128)(2,1)S(1)}, bf16[256,512]{1,0:T(8,128)(2,1)}, u32[]{:S(2)}) copy-start(bf16[256,512]{1,0:T(8,128)(2,1)} %param.24) | copy-start | bytes 786436
  116.4 41.8 %copy-start.11 = (bf16[256,512]{1,0:T(8,128)(2,1)S(1)}, bf16[256,512]{1,0:T(8,128)(2,1)}, u32[]{:S(2)}) copy-start(bf16[256,512]{1,0:T(8,128)(2,1)} %param.25) | copy-start | bytes 786436
  155.0 3.3 %copy-start.5 = (f32[256,512]{1,0:T(8,128)S(1)}, f32[256,512]{1,0:T(8,128)}, u32[]{:S(2)}) copy-start(f32[256,512]{1,0:T(8,128)} %get-tuple-element.19) | copy-start | bytes 1572868
where the time goes:
time: 160 us; the launch traced here: 159 us
  Pallas kernels  119 us (74%)
  matrix products  23.9 us (15%)
  other arithmetic  9.92 us (6%)
  local copies, waits for them, and re-layouts  5.54 us (3%)
    pallas_call x1, Pallas kernels, dispatch(): pl.pallas_call(functools.partial(dispatch_kernel, group, narrow, width),...  39.1 us
    pallas_call x1, Pallas kernels, tail(): pl.pallas_call(functools.partial(tail_kernel, group, narrow, reach), out_...  38.6 us
    pallas_call x1, Pallas kernels, return_home(): pl.pallas_call(functools.partial(return_kernel, group, narrow, width), ou...  30 us
    pallas_call x1, Pallas kernels, widen(): pl.pallas_call(functools.partial(widen_kernel, narrow, width, pieces), ou...  11.3 us
    dot_general x1, matrix products, per_device(): jnp.dot(rows_in.T, d_gate, preferred_element_type=f32).astype(bf16)  3.94 us
    unnamed x38, local copies, waits for them, and re-layouts  3.93 us
    dot_general x1, matrix products, per_device(): d_act = jnp.dot(rows_cot, down_weight.T, preferred_element_type=f32)  3.89 us

commit v1 on v0

--- a/solution.py
+++ b/solution.py
@@ -53,192 +53,339 @@
     pl.semaphore_wait(barrier, len(peers))
 
 
-def dispatch_kernel(
+def dots(lhs, rhs, left, right):
+    return lax.dot_general(lhs, rhs, (((left,), (right,)), ((), ())), preferred_element_type=jnp.float32)
+
+
+def expert_kernel(
     group,
     narrow,
-    width,
+    cap,
+    ids_hbm,
+    weight_hbm,
+    cot_hbm,
+    conv_hbm,
+    rows_hbm,
+    gate_hbm,
+    up_hbm,
+    down_hbm,
+    mix_ref,
+    stats_ref,
+    gate_out,
+    up_out,
+    down_out,
+    ids_ref,
+    weight_ref,
+    cot_ref,
+    conv_ref,
+    in_ref,
+    pair_w,
+    down_ref,
     out_ref,
+    cot_rows,
+    act_ref,
+    up_slope,
+    gate_slope,
+    delta,
+    part,
+    pair_buf,
+    far_out,
+    far_in,
+    done,
+    home,
     stat_ref,
-    in_ref,
-    gate_ref,
-    up_ref,
-    rows_ref,
-    stats_ref,
-    gate_lin_ref,
-    up_lin_ref,
     *sems,
 ):
-    a_s, a_r, n_s, n_r, f_s, f_r, m_s, m_r, t_s, t_r, l_s = sems
+    a_s, a_r, n_s, n_r, f_s, f_r, m_s, m_r, pn_s, pn_r, pf_s, pf_r, h_s, h_r, t_s, t_r, l_s = sems
+    f32, bf16 = jnp.float32, jnp.bfloat16
     me, t, near, far, cross = places(group, narrow)
     partner, across = around(me, group, 1)
+    arriving = around(me, group, -1)[1]
     sp_peers = [partner] + across
-    meet([(p, t) for p in sp_peers] + [(me, near), (me, far), (me, cross)])
+    peers = [(p, t) for p in sp_peers] + [(me, near), (me, far), (me, cross)]
+    barrier = pltpu.get_barrier_semaphore()
+    for sp, tp in peers:
+        pl.semaphore_signal(barrier, inc=1, device_id=(sp, tp), device_id_type=MESH)
+
+    tokens, width = cot_ref.shape
+    slots, model = cot_rows.shape
+    hidden = down_ref.shape[0]
+    chosen = ids_ref.shape[1]
+    loads = [
+        pltpu.make_async_copy(s, d, l_s.at[k])
+        for k, (s, d) in enumerate(
+            [
+                (ids_hbm, ids_ref),
+                (weight_hbm, weight_ref),
+                (cot_hbm, cot_ref),
+                (conv_hbm, conv_ref),
+                (rows_hbm, in_ref),
+                (gate_hbm, pair_w.at[:, pl.ds(0, hidden)]),
+                (up_hbm, pair_w.at[:, pl.ds(hidden, hidden)]),
+                (down_hbm, down_ref),
+            ]
+        )
+    ]
+    for c in loads:
+        c.start()
+    for c in loads[:3]:
+        c.wait()
+
+    ids = ids_ref[...]
+    lane = lax.broadcasted_iota(jnp.int32, (tokens, 128), 1)
+    spread_ids = jnp.zeros((tokens, 128), f32)
+    for k in range(chosen):
+        spread_ids = jnp.where(lane == k, ids[:, k : k + 1].astype(f32), spread_ids)
+    ids_rows = jnp.transpose(spread_ids)[:8].astype(jnp.int32)
+    experts = -(-group // 8) * 8
+    expert = lax.broadcasted_iota(jnp.int32, (experts, tokens), 0)
+    hots = [ids_rows[k : k + 1] == expert for k in range(chosen)]
+    hot = functools.reduce(jnp.logical_or, hots).astype(f32).astype(bf16)
+    first = lax.broadcasted_iota(jnp.int32, (tokens, tokens), 0)
+    second = lax.broadcasted_iota(jnp.int32, (tokens, tokens), 1)
+    earlier = dots(hot, (first < second).astype(f32).astype(bf16), 1, 0)
+    slot_row = lax.broadcasted_iota(jnp.int32, (slots, tokens), 0)
+    picks = []
+    outgoing = jnp.zeros((slots, width), f32)
+    for k in range(chosen):
+        slot = jnp.sum(jnp.where(hots[k], earlier, 0.0), axis=0, keepdims=True).astype(jnp.int32)
+        dest = ids_rows[k : k + 1] * cap + slot
+        pick = (slot_row == dest).astype(f32).astype(bf16)
+        scaled = (weight_ref[:, k : k + 1] * cot_ref[...].astype(f32)).astype(bf16)
+        outgoing = outgoing + dots(pick, scaled, 1, 0)
+        picks.append(pick)
+    out_ref[...] = outgoing.astype(bf16)
+    pick_any = functools.reduce(jnp.add, picks)
+
+    def block(s):
+        return pl.ds(pl.multiple_of(s * cap, cap), cap)
 
     def spot(s, column):
-        return rows_ref.at[s, :, lanes(column, width)]
+        return cot_rows.at[block(s), lanes(column, width)]
+
+    cot_rows[block(me), lanes(t, width)] = out_ref[block(me), :]
+    pl.semaphore_wait(barrier, len(peers))
 
     def swap(s):
-        return remote(out_ref.at[s], spot(me, t), a_s.at[s], a_r.at[me], s, t)
-
-    for p in sp_peers:
-        swap(p).start()
-    stat_own = pltpu.make_async_copy(stat_ref, stats_ref.at[t], l_s.at[0])
-    stat_own.start()
+        return remote(out_ref.at[block(s)], spot(me, t), a_s.at[s], a_r.at[me], s, t)
+
+    def to_far(s):
+        return remote(spot(s, t), spot(s, t), f_s.at[s], f_r.at[s], me, far)
+
+    def to_near(s):
+        return remote(spot(s, t), spot(s, t), n_s.at[s], n_r.at[s], me, near)
+
+    def onward(s):
+        return remote(spot(s, far), spot(s, far), m_s.at[s], m_r.at[s], me, near)
+
+    def part_near(s, k):
+        column = near if k == 0 else cross
+        return remote(
+            part.at[block(s), lanes(column, width)],
+            pair_buf.at[k, block(s)],
+            pn_s.at[s, k],
+            pn_r.at[s, k],
+            me,
+            near,
+        )
+
+    def part_far(s):
+        return remote(far_out.at[block(s)], far_in.at[block(s)], pf_s.at[s], pf_r.at[s], me, far)
+
+    def to_home(s):
+        return remote(done.at[block(s)], home.at[block(me)], h_s.at[s], h_r.at[me], s, t)
+
+    def from_home(s):
+        return remote(done.at[block(s)], home.at[block(s)], h_s.at[s], h_r.at[s], s, t)
+
+    def arrive(s):
+        remote(out_ref.at[block(s)], spot(s, t), a_s.at[s], a_r.at[s], s, t).wait_recv()
+
+    def fan(s):
+        to_far(s).start()
+        to_near(s).start()
+
+    def relay(s):
+        to_far(s).wait_recv()
+        onward(s).start()
+
+    def slopes(piece, pieces):
+        count = slots // pieces
+        span = pl.ds(piece * count, count)
+        both = jnp.dot(in_ref[span, :], pair_w[...], preferred_element_type=f32)
+        gate_lin, up_lin = both[:, :hidden], both[:, hidden:]
+        gate_c = jnp.minimum(gate_lin, clamp_limit)
+        up_c = jnp.clip(up_lin, -clamp_limit, clamp_limit)
+        sigma = jax.nn.sigmoid(swish_alpha * gate_c)
+        lift, gated = up_c + 1.0, gate_c * sigma
+        act_ref[span, :] = (lift * gated).astype(bf16)
+        up_open = (up_lin > -clamp_limit) & (up_lin < clamp_limit)
+        up_slope[span, :] = jnp.where(up_open, gated, 0.0)
+        slope = lift * (sigma + swish_alpha * gated * (1.0 - sigma))
+        gate_slope[span, :] = jnp.where(gate_lin < clamp_limit, slope, 0.0)
+
+    def compute(s, ready):
+        rows = block(s)
+        if not ready:
+            remote(spot(s, near), spot(s, near), n_s.at[s], n_r.at[s], me, near).wait_recv()
+            remote(spot(s, cross), spot(s, cross), m_s.at[s], m_r.at[s], me, near).wait_recv()
+        d_act = dots(cot_rows[rows, :], down_ref[...], 1, 1)
+        d_gate = (d_act * gate_slope[rows, :]).astype(bf16)
+        d_up = (d_act * up_slope[rows, :]).astype(bf16)
+        delta[rows, pl.ds(0, hidden)] = d_gate
+        delta[rows, pl.ds(hidden, hidden)] = d_up
+        cut = min(model, 1024)
+        for j in range(model // cut):
+            span = pl.ds(j * cut, cut)
+            part[rows, span] = dots(delta[rows, :], pair_w[span, :], 1, 1).astype(bf16)
+        part_near(s, 1).start()
+        part_near(s, 0).start()
+
+    def pair_up(s):
+        rows = block(s)
+        part_near(s, 1).wait_recv()
+        pair = part[rows, lanes(far, width)].astype(f32) + pair_buf[1, rows].astype(f32)
+        far_out[rows, :] = pair.astype(bf16)
+        part_far(s).start()
+
+    def finish(s, own):
+        rows = block(s)
+        part_near(s, 0).wait_recv()
+        part_far(s).wait_recv()
+        total = part[rows, lanes(t, width)].astype(f32)
+        total = total + pair_buf[0, rows].astype(f32) + far_in[rows, :].astype(f32)
+        if own:
+            home[rows, :] = total.astype(bf16)
+        else:
+            done[rows, :] = total.astype(bf16)
+            to_home(s).start()
+
+    for s in across + [partner]:
+        swap(s).start()
+    fan(me)
+    loads[3].wait()
+    conv = conv_ref[...].astype(f32)
+    sums = jnp.where(lane == 0, jnp.sum(conv, axis=1, keepdims=True), 0.0)
+    sums = jnp.where(lane == 1, jnp.sum(conv * conv, axis=1, keepdims=True), sums)
+    stat_ref[...] = jnp.transpose(sums)[:8]
     small = []
     for k, p in enumerate((near, far, cross)):
         c = remote(stat_ref, stats_ref.at[t], t_s.at[k], t_r.at[k], me, p)
         c.start()
         small.append(c)
-    own = pltpu.make_async_copy(out_ref.at[me], spot(me, t), l_s.at[1])
-    own.start()
-    own.wait()
-    order = [me, partner] + around(me, group, -1)[1]
-
-    def to_far(s):
-        return remote(spot(s, t), spot(s, t), f_s.at[s], f_r.at[s], me, far)
-
-    def to_near(s):
-        return remote(spot(s, t), spot(s, t), n_s.at[s], n_r.at[s], me, near)
-
-    def onward(s):
-        return remote(spot(s, far), spot(s, far), m_s.at[s], m_r.at[s], me, near)
-
-    def relay(s):
-        to_far(s).wait_recv()
-        onward(s).start()
-
-    turns = 8
-    count = in_ref.shape[0] // turns
-
-    def multiply(piece):
-        span = pl.ds(piece * count, count)
-        rows = in_ref[span, :]
-        gate_lin_ref[span, :] = jnp.dot(rows, gate_ref[...], preferred_element_type=jnp.float32)
-        up_lin_ref[span, :] = jnp.dot(rows, up_ref[...], preferred_element_type=jnp.float32)
-
-    lag = min(2, group)
-    for i, s in enumerate(order):
-        if i > 0:
-            remote(out_ref.at[s], spot(s, t), a_s.at[s], a_r.at[s], s, t).wait_recv()
-        to_far(s).start()
-        to_near(s).start()
-        if i >= lag:
-            relay(order[i - lag])
-        for piece in range(turns * i // group, turns * (i + 1) // group):
-            multiply(piece)
-    for s in order[group - lag :]:
-        relay(s)
-    for s in order:
+    stats_ref[t] = stat_ref[...]
+    for c in loads[4:]:
+        c.wait()
+    pieces = 4
+    slopes(0, pieces)
+    arrive(partner)
+    fan(partner)
+    relay(me)
+    fill = [functools.partial(slopes, p, pieces) for p in range(1, pieces)]
+    count = len(arriving)
+
+    def at(k):
+        return arriving[k]
+
+    for i in range(count + 5):
+        if i - 5 >= 0 and i - 5 < count:
+            finish(at(i - 5), False)
+        if 0 <= i - 3 < count:
+            pair_up(at(i - 3))
+        if 0 <= i - 2 < count:
+            compute(at(i - 2), False)
+        if i < count:
+            arrive(at(i))
+            fan(at(i))
+        if i == 0:
+            relay(partner)
+        elif i - 1 < count:
+            relay(at(i - 1))
+        for _ in range(2 - i):
+            fill.pop(0)()
+        if i == count:
+            compute(partner, False)
+            compute(me, False)
+        if i == count + 2:
+            pair_up(partner)
+            pair_up(me)
+            down_out[...] = dots(act_ref[...], cot_rows[...], 0, 0).astype(bf16)
+        if i == count + 3:
+            gate_out[...] = dots(in_ref[...], delta[:, :hidden], 0, 0).astype(bf16)
+        if i == count + 4:
+            up_out[...] = dots(in_ref[...], delta[:, hidden:], 0, 0).astype(bf16)
+    finish(partner, False)
+    finish(me, True)
+    for s in sp_peers:
+        from_home(s).wait_recv()
+    summed = dots(pick_any, home[...], 0, 0)
+    mix_ref[...] = (cot_ref[...].astype(f32) + summed).astype(bf16)
+    for s in [me] + sp_peers:
         to_far(s).wait_send()
         to_near(s).wait_send()
         onward(s).wait_send()
-        remote(spot(s, near), spot(s, near), n_s.at[s], n_r.at[s], me, near).wait_recv()
-        remote(spot(s, cross), spot(s, cross), m_s.at[s], m_r.at[s], me, near).wait_recv()
-    for p in sp_peers:
-        swap(p).wait_send()
-    stat_own.wait()
+        part_near(s, 0).wait_send()
+        part_near(s, 1).wait_send()
+        part_far(s).wait_send()
+    for s in sp_peers:
+        swap(s).wait_send()
+        to_home(s).wait_send()
     for c in small:
         c.wait_send()
         c.wait_recv()
 
 
-def dispatch(outgoing, stat, rows_in, gate_weight, up_weight):
-    group, capacity, width = outgoing.shape
-    narrow = lax.axis_size("tp")
+def expert_pass(ids, weight, cot, conv, rows_in, gate_weight, up_weight, down_weight):
+    group, narrow = lax.axis_size("sp"), lax.axis_size("tp")
+    tokens, width = cot.shape
+    slots, model = rows_in.shape
+    hidden = down_weight.shape[0]
+    cap = slots // group
+    f32, bf16 = jnp.float32, jnp.bfloat16
     dma = pltpu.SemaphoreType.DMA
+    rows = (slots, width)
     return pl.pallas_call(
-        functools.partial(dispatch_kernel, group, narrow, width),
+        functools.partial(expert_kernel, group, narrow, cap),
         out_shape=(
-            jax.ShapeDtypeStruct((group, capacity, narrow * width), outgoing.dtype),
-            jax.ShapeDtypeStruct((narrow,) + stat.shape, stat.dtype),
-            jax.ShapeDtypeStruct((rows_in.shape[0], gate_weight.shape[1]), jnp.float32),
-            jax.ShapeDtypeStruct((rows_in.shape[0], up_weight.shape[1]), jnp.float32),
+            jax.ShapeDtypeStruct((tokens, width), bf16),
+            jax.ShapeDtypeStruct((narrow, 8, tokens), f32),
+            jax.ShapeDtypeStruct((model, hidden), bf16),
+            jax.ShapeDtypeStruct((model, hidden), bf16),
+            jax.ShapeDtypeStruct((hidden, model), bf16),
         ),
-        in_specs=[pl.BlockSpec(memory_space=VMEM)] * 5,
-        out_specs=[pl.BlockSpec(memory_space=VMEM)] * 4,
-        scratch_shapes=[dma((group,))] * 8 + [dma((3,))] * 2 + [dma((2,))],
-        compiler_params=pltpu.CompilerParams(collective_id=0, has_side_effects=True),
-    )(outgoing, stat, rows_in, gate_weight, up_weight)
-
-
-def return_kernel(group, narrow, width, part_ref, home_ref, pair_buf, far_out, far_in, done, *sems):
-    n_s, n_r, f_s, f_r, a_s, a_r, l_s = sems
-    me, t, near, far, cross = places(group, narrow)
-    partner, across = around(me, group, 1)
-    sp_peers = across + [partner]
-    meet([(p, t) for p in sp_peers] + [(me, near), (me, far)])
-    order = sp_peers + [me]
-
-    def part(s, column):
-        return part_ref.at[s, :, lanes(column, width)]
-
-    def to_near(s, k):
-        return remote(
-            part(s, near if k == 0 else cross), pair_buf.at[s, k], n_s.at[s, k], n_r.at[s, k], me, near
-        )
-
-    def to_far(s):
-        return remote(far_out.at[s], far_in.at[s], f_s.at[s], f_r.at[s], me, far)
-
-    def to_home(s):
-        return remote(done.at[s], home_ref.at[me], a_s.at[s], a_r.at[me], s, t)
-
-    for s in order:
-        to_near(s, 1).start()
-    for s in order:
-        to_near(s, 0).start()
-    own = pltpu.make_async_copy(done.at[me], home_ref.at[me], l_s.at[0])
-
-    def finish(s, i):
-        to_near(s, 0).wait_recv()
-        to_far(s).wait_recv()
-        total = part_ref[s, :, lanes(t, width)].astype(jnp.float32)
-        total = total + pair_buf[s, 0].astype(jnp.float32) + far_in[s].astype(jnp.float32)
-        done[s] = total.astype(done.dtype)
-        if i < group - 1:
-            to_home(s).start()
-        else:
-            own.start()
-
-    for s in order:
-        to_near(s, 1).wait_recv()
-        pair = part_ref[s, :, lanes(far, width)].astype(jnp.float32) + pair_buf[s, 1].astype(jnp.float32)
-        far_out[s] = pair.astype(far_out.dtype)
-        to_far(s).start()
-    for i, s in enumerate(order):
-        finish(s, i)
-    own.wait()
-    for s in order:
-        to_near(s, 0).wait_send()
-        to_near(s, 1).wait_send()
-        to_far(s).wait_send()
-    for s in sp_peers:
-        to_home(s).wait_send()
-        remote(done.at[s], home_ref.at[s], a_s.at[s], a_r.at[s], s, t).wait_recv()
-
-
-def return_home(partial):
-    group, capacity, whole = partial.shape
-    narrow = lax.axis_size("tp")
-    width = whole // narrow
-    dma = pltpu.SemaphoreType.DMA
-    block = (group, capacity, width)
-    return pl.pallas_call(
-        functools.partial(return_kernel, group, narrow, width),
-        out_shape=jax.ShapeDtypeStruct(block, partial.dtype),
-        in_specs=[pl.BlockSpec(memory_space=VMEM)],
-        out_specs=pl.BlockSpec(memory_space=VMEM),
+        in_specs=[pl.BlockSpec(memory_space=pl.ANY)] * 8,
+        out_specs=[pl.BlockSpec(memory_space=VMEM)] * 5,
         scratch_shapes=[
-            VMEM((group, 2, capacity, width), partial.dtype),
-            VMEM(block, partial.dtype),
-            VMEM(block, partial.dtype),
-            VMEM(block, partial.dtype),
+            VMEM(ids.shape, ids.dtype),
+            VMEM(weight.shape, weight.dtype),
+            VMEM(cot.shape, bf16),
+            VMEM(conv.shape, bf16),
+            VMEM(rows_in.shape, bf16),
+            VMEM((model, 2 * hidden), bf16),
+            VMEM(down_weight.shape, bf16),
+            VMEM(rows, bf16),
+            VMEM((slots, model), bf16),
+            VMEM((slots, hidden), bf16),
+            VMEM((slots, hidden), f32),
+            VMEM((slots, hidden), f32),
+            VMEM((slots, 2 * hidden), bf16),
+            VMEM((slots, model), bf16),
+            VMEM((2,) + rows, bf16),
+            VMEM(rows, bf16),
+            VMEM(rows, bf16),
+            VMEM(rows, bf16),
+            VMEM(rows, bf16),
+            VMEM((8, tokens), f32),
         ]
+        + [dma((group,))] * 8
         + [dma((group, 2))] * 2
         + [dma((group,))] * 4
-        + [dma((1,))],
-        compiler_params=pltpu.CompilerParams(collective_id=1, has_side_effects=True),
-    )(partial)
+        + [dma((3,))] * 2
+        + [dma((8,))],
+        compiler_params=pltpu.CompilerParams(
+            collective_id=0, has_side_effects=True, vmem_limit_bytes=60 * 1024 * 1024
+        ),
+    )(ids, weight, cot, conv, rows_in, gate_weight, up_weight, down_weight)
 
 
 def widen_kernel(narrow, width, pieces, mix_ref, full_ref, *sems):
@@ -489,65 +636,22 @@
     group_size = lax.axis_size("sp")
     narrow_size = lax.axis_size("tp")
     tok_rows, local_cols = cot_out.shape
-    chosen = route_ids.shape[1]
-    slot_rows = expert_inputs.shape[1]
+    f32, bf16 = jnp.float32, jnp.bfloat16
+    convolution_filter = conv_out.astype(f32)
+    rows_in = expert_inputs[0]
+    slot_rows, model_width = rows_in.shape
     capacity = slot_rows // group_size
-    model_width = expert_inputs.shape[2]
-    f32, bf16 = jnp.float32, jnp.bfloat16
-    experts = jnp.arange(group_size, dtype=jnp.int32)[None, :]
-    hots = [(route_ids[:, k : k + 1] == experts) for k in range(chosen)]
-    hot = functools.reduce(jnp.logical_or, hots)
-    token = jnp.arange(tok_rows, dtype=jnp.int32)
-    before = (token[:, None] > token[None, :]).astype(bf16)
-    earlier = jnp.dot(before, hot.astype(bf16), preferred_element_type=f32)
-    slots = jnp.arange(slot_rows, dtype=jnp.int32)[None, :]
-    picks, scaled = [], []
-    for k in range(chosen):
-        slot = jnp.sum(jnp.where(hots[k], earlier, 0.0), axis=1).astype(jnp.int32)
-        dest = route_ids[:, k] * capacity + slot
-        picks.append((dest[:, None] == slots).astype(bf16))
-        scaled.append((route_weight[:, k : k + 1] * cot_out.astype(f32)).astype(bf16))
-    outgoing = lax.dot_general(
-        jnp.concatenate(picks, axis=0),
-        jnp.concatenate(scaled, axis=0),
-        (((0,), (0,)), ((), ())),
-        preferred_element_type=f32,
-    ).astype(bf16)
-    convolution_filter = conv_out.astype(f32)
-    stat = jnp.stack(
-        [jnp.sum(convolution_filter, axis=1), jnp.sum(convolution_filter * convolution_filter, axis=1)]
+    fitted = -(-capacity // 16) * 16
+    if fitted != capacity:
+        rows_in = rows_in.reshape(group_size, capacity, model_width)
+        rows_in = jnp.pad(rows_in, ((0, 0), (0, fitted - capacity), (0, 0)))
+        rows_in = rows_in.reshape(group_size * fitted, model_width)
+    mix_grad, stats, grad_gate_part, grad_up_part, grad_down = expert_pass(
+        route_ids, route_weight, cot_out, conv_out, rows_in, w_gate[0], w_up[0], w_down[0]
     )
-    rows_in = expert_inputs[0]
-    gate_weight = w_gate[0]
-    up_weight = w_up[0]
-    down_weight = w_down[0]
-    arrived, stats, gate_lin, up_lin = dispatch(
-        outgoing.reshape(group_size, capacity, local_cols), stat, rows_in, gate_weight, up_weight
-    )
-    rows_cot = arrived.reshape(slot_rows, model_width)
-    gate_c = jnp.minimum(gate_lin, clamp_limit)
-    up_c = jnp.clip(up_lin, -clamp_limit, clamp_limit)
-    sigma = jax.nn.sigmoid(swish_alpha * gate_c)
-    act = ((up_c + 1.0) * gate_c * sigma).astype(bf16)
-    grad_down = jnp.dot(act.T, rows_cot, preferred_element_type=f32).astype(bf16)
-    d_act = jnp.dot(rows_cot, down_weight.T, preferred_element_type=f32)
-    up_open = ((up_lin > -clamp_limit) & (up_lin < clamp_limit)).astype(f32)
-    gate_open = (gate_lin < clamp_limit).astype(f32)
-    d_up = (d_act * gate_c * sigma * up_open).astype(bf16)
-    d_gate = (
-        d_act * (up_c + 1.0) * (sigma + swish_alpha * gate_c * sigma * (1.0 - sigma)) * gate_open
-    ).astype(bf16)
-    grad_gate_part = jnp.dot(rows_in.T, d_gate, preferred_element_type=f32).astype(bf16)
-    grad_up_part = jnp.dot(rows_in.T, d_up, preferred_element_type=f32).astype(bf16)
-    partial_value = jnp.dot(d_gate, gate_weight.T, preferred_element_type=f32)
-    partial_value = partial_value + jnp.dot(d_up, up_weight.T, preferred_element_type=f32)
-    coming = return_home(partial_value.astype(bf16).reshape(group_size, capacity, model_width))
-    pick_any = functools.reduce(jnp.add, picks)
-    summed = jnp.dot(pick_any, coming.reshape(slot_rows, local_cols), preferred_element_type=f32)
-    mix_grad = (cot_out.astype(f32) + summed).astype(bf16)
     mix_full = widen(mix_grad)
     channel_total = local_cols * narrow_size
-    first_sum, square_sum = jnp.sum(stats, axis=0)
+    first_sum, square_sum = jnp.sum(stats, axis=0)[:2]
     channel_mean = (first_sum / channel_total)[:, None]
     var = (square_sum / channel_total)[:, None] - channel_mean * channel_mean
     inverse_deviation = lax.rsqrt(var + norm_epsilon)

time: 160 us -> 130 us (0.81)
  matrix products: 23.9 us -> 5.37 us
  Pallas kernels: 119 us -> 111 us
  other arithmetic: 9.92 us -> 5.73 us
    dot_general x9 -> x0, matrix products: 18.6 us -> none  [the longest x1 3.94 us: per_device(): jnp.dot(rows_in.T, d_gate, preferred_element_type=f32).astype(bf16)]
    pallas_call x2 -> x1, Pallas kernels: 69.1 us -> 62.7 us  [expert_pass(): pl.pallas_call(functools.partial(expert_kernel, group, narrow, cap), out_...]
    unnamed x38 -> x25, local copies, waits for them, and re-layouts: 3.93 us -> 6.06 us
    slice x2 -> x0, local copies, waits for them, and re-layouts: 1.61 us -> none  [the longest x1 0.85 us: per_device(): scaled.append((route_weight[:, k:k + 1] * cot_out.astype(f32)).astype(bf16))]
where the time goes in v1:
time: 130 us; the launch traced here: 129 us
  Pallas kernels  111 us (85%)
  local copies, waits for them, and re-layouts  6.06 us (5%)
  other arithmetic  5.73 us (4%)
  matrix products  5.37 us (4%)
    pallas_call x1, Pallas kernels, expert_pass(): pl.pallas_call(functools.partial(expert_kernel, group, narrow, cap), out_...  62.7 us
    pallas_call x1, Pallas kernels, tail(): pl.pallas_call(functools.partial(tail_kernel, group, narrow, reach), out_...  38 us
    pallas_call x1, Pallas kernels, widen(): pl.pallas_call(functools.partial(widen_kernel, narrow, width, pieces), ou...  10.5 us
    unnamed x25, local copies, waits for them, and re-layouts  6.06 us
    dot_general x1, matrix products, per_device(): d_act_conv = jnp.dot(mix_full, w_proj.T, preferred_element_type=f32)  3.09 us

profile of v1, /device:TPU:0, one launch (start us, length us, event | category | flops | bytes accessed | tf_op | source)
XLA Modules:
  0.0 129.2 jit_solution(4509911112936288105)
XLA Ops:
  0.6 0.0 copy-start
  0.6 1.6 %copy.19.ids_hbm = s32[256,2]{1,0:T(8,128)} copy(s32[256,2]{0,1:T(2,128)} %param.14) | data formatting | bytes 4096 | tf_op args[1]
  2.3 1.5 %copy.20.weight_hbm = f32[256,2]{1,0:T(8,128)} copy(f32[256,2]{0,1:T(2,128)} %param.15) | data formatting | bytes 4096 | tf_op args[2]
  3.7 0.0 copy-start.6
  3.7 0.0 copy-start.9
  3.8 62.7 %shard_map.172 = (bf16[256,512]{1,0:T(8,128)(2,1)}, f32[4,8,256]{2,1,0:T(8,128)}, bf16[2048,256]{1,0:T(8,128)(2,1)}, bf16[2048,256]{1,0:T(8,128)(2,1)}, bf16[256,2048]{1,0:T(8,128)(2,1)}) custom-call(s32[256,2]{1,0:T(8,128)} %copy.19.ids_hbm, f32[256,2]{1,0:T(8,128)} %copy.20.weight_hbm, bf16[256,512]{1,0:T(8,128)(2,1)} %cot_hbm.1, ...), custom_call_target="tpu_custom_call" | custom-call | tf_op jit(solution)/shard_map/pallas_call | solution.py:347
  66.5 0.8 reduce_sum.36
  67.3 10.5 %shard_map.173 = bf16[256,2048]{1,0:T(8,128)(2,1)} custom-call(bf16[256,512]{1,0:T(8,128)(2,1)} %get-tuple-element.18.mix_ref), custom_call_target="tpu_custom_call" | custom-call | tf_op jit(solution)/shard_map/pallas_call | solution.py:433
  77.8 0.0 copy-done
  77.8 0.0 copy-done.6
  77.9 0.0 copy-done.9
  77.9 0.0 copy-start.1
  77.9 3.1 %fusion.5 = (f32[256]{0:T(256)S(1)}, f32[256]{0:T(256)S(1)}, f32[256,512]{1,0:T(8,128)}, f32[256,512]{1,0:T(8,128)}) fusion(f32[256]{0:T(256)S(1)} %add_rsqrt_fusion.1, f32[256]{0:T(256)S(1)} %bitcast.24, bf16[256,512]{1,0:T(8,128)(2,1)S(1)} %copy-done.6, f32[512]{0:T(512)S(1)} %copy-done.9, bf16[256,2048]{1,0:T(8,128)(2,1)} %shard_map.173, ...), kind=kOutput, calls=%fused_computation.22 | convolution fusion | flops 538967552 | bytes 4462592 | tf_op jit(solution)/shard_map/dot_general | solution.py:665
  81.0 0.6 select_maximum_fusion.stat_ref
  81.6 0.0 copy-done.1
  81.6 2.3 %convolution_convert_fusion = bf16[512,2048]{1,0:T(8,128)(2,1)} fusion(bf16[256,2048]{1,0:T(8,128)(2,1)S(1)} %copy-done.1, f32[512]{0:T(512)S(1)} %copy-done.9, bf16[256,512]{1,0:T(8,128)(2,1)S(1)} %copy-done.6, f32[256]{0:T(256)S(1)} %add_rsqrt_fusion.1, f32[256]{0:T(256)S(1)} %bitcast.25), kind=kOutput, calls=%fused_computation | convolution fusion | flops 539099136 | bytes 3411968 | tf_op jit(solution)/shard_map/dot_general | solution.py:662
  83.9 38.0 %shard_map.174 = (f32[64,2048]{1,0:T(8,128)}, bf16[3,64,2048]{2,1,0:T(8,128)(2,1)}, f32[256,512]{1,0:T(8,128)}) custom-call(bf16[8,64,2048]{2,1,0:T(8,128)(2,1)} %bitcast.16, f32[256,512]{1,0:T(8,128)} %get-tuple-element.30.grad_ref, f32[256,512]{1,0:T(8,128)} %get-tuple-element.26.hat_ref, f32[8,256]{1,0:T(8,128)} %select_maximum_fusion.stat_ref, ...), custom_call_target="tpu_custom_call" | custom-call | tf_op jit(solution)/shard_map/pallas_call | solution.py:592
  121.9 0.0 copy-start.5
  121.9 0.0 copy-start.7
  121.9 0.0 copy-start.8
  121.9 0.0 copy-start.4
  121.9 1.4 %convert_reduce_fusion = f32[64,2048]{1,0:T(8,128)S(1)} fusion(bf16[3,64,2048]{2,1,0:T(8,128)(2,1)} %get-tuple-element.20), kind=kLoop, calls=%fused_computation.1 | loop fusion | flops 655360 | bytes 1310720 | tf_op jit(solution)/shard_map/reduce_sum | solution.py:687
  123.4 1.9 %add.36 = f32[64,2048]{1,0:T(8,128)} add(f32[64,2048]{1,0:T(8,128)} %get-tuple-element.19, f32[64,2048]{1,0:T(8,128)S(1)} %convert_reduce_fusion) | non-fusion elementwise | flops 131072 | bytes 1572864 | tf_op jit(solution)/shard_map/add | solution.py:687
  125.3 0.0 copy-done.5
  125.3 0.0 copy-done.7
  125.3 0.0 copy-done.8
  125.3 0.0 copy-start.3
  125.3 1.0 multiply_convert_fusion
  126.3 0.0 copy-done.4
  126.3 0.0 copy-start.2
  126.3 1.0 copy.24
  127.3 0.0 copy-done.3
  127.3 1.0 copy.25
  128.2 0.0 copy-done.2
  128.2 1.0 copy.26
  (2 shorter events, 0.0 us)
Async XLA Ops:
  0.6 77.2 %copy-start = (bf16[512,2048]{1,0:T(8,128)(2,1)S(1)}, bf16[512,2048]{1,0:T(8,128)(2,1)}, u32[]{:S(2)}) copy-start(bf16[512,2048]{1,0:T(8,128)(2,1)} %param.20) | copy-start | bytes 6291460
  3.7 74.1 %copy-start.6 = (bf16[256,512]{1,0:T(8,128)(2,1)S(1)}, bf16[256,512]{1,0:T(8,128)(2,1)}, u32[]{:S(2)}) copy-start(bf16[256,512]{1,0:T(8,128)(2,1)} %conv_hbm.1) | copy-start | bytes 786436
  3.7 74.1 %copy-start.9 = (f32[512]{0:T(512)S(1)}, f32[512]{0:T(512)}, u32[]{:S(2)}) copy-start(f32[512]{0:T(512)} %param.22) | copy-start | bytes 6148
  77.9 3.7 %copy-start.1 = (bf16[256,2048]{1,0:T(8,128)(2,1)S(1)}, bf16[256,2048]{1,0:T(8,128)(2,1)}, u32[]{:S(2)}) copy-start(bf16[256,2048]{1,0:T(8,128)(2,1)} %shard_map.173) | copy-start | bytes 3145732
  121.9 3.4 %copy-start.5 = (f32[256,512]{1,0:T(8,128)S(1)}, f32[256,512]{1,0:T(8,128)}, u32[]{:S(2)}) copy-start(f32[256,512]{1,0:T(8,128)} %get-tuple-element.21) | copy-start | bytes 1572868
  121.9 3.4 %copy-start.7 = (bf16[256,512]{1,0:T(8,128)(2,1)S(1)}, bf16[256,512]{1,0:T(8,128)(2,1)}, u32[]{:S(2)}) copy-start(bf16[256,512]{1,0:T(8,128)(2,1)} %param.24) | copy-start | bytes 786436
  121.9 3.4 %copy-start.8 = (bf16[256,512]{1,0:T(8,128)(2,1)S(1)}, bf16[256,512]{1,0:T(8,128)(2,1)}, u32[]{:S(2)}) copy-start(bf16[256,512]{1,0:T(8,128)(2,1)} %param.25) | copy-start | bytes 786436
  121.9 4.4 %copy-start.4 = (bf16[2048,256]{1,0:T(8,128)(2,1)S(1)}, bf16[2048,256]{1,0:T(8,128)(2,1)}, u32[]{:S(2)}) copy-start(bf16[2048,256]{1,0:T(8,128)(2,1)} %get-tuple-element.14) | copy-start | bytes 3145732
  125.3 2.0 %copy-start.3 = (bf16[2048,256]{1,0:T(8,128)(2,1)S(1)}, bf16[2048,256]{1,0:T(8,128)(2,1)}, u32[]{:S(2)}) copy-start(bf16[2048,256]{1,0:T(8,128)(2,1)} %get-tuple-element.15) | copy-start | bytes 3145732
  126.3 1.9 %copy-start.2 = (bf16[256,2048]{1,0:T(8,128)(2,1)S(1)}, bf16[256,2048]{1,0:T(8,128)(2,1)}, u32[]{:S(2)}) copy-start(bf16[256,2048]{1,0:T(8,128)(2,1)} %get-tuple-element.16) | copy-start | bytes 3145732

commit v2 on v1

v2 whole, which is shorter than its diff:
```python
import functools

import jax
import jax.numpy as jnp
from jax import lax
from jax.experimental import pallas as pl
from jax.experimental.pallas import tpu as pltpu
from jax.sharding import PartitionSpec as P

clamp_limit = 7.0
swish_alpha = 1.702
norm_epsilon = 1e-05
MESH = pl.DeviceIdType.MESH
VMEM = pltpu.VMEM


def lanes(index, width):
    return pl.ds(pl.multiple_of(index * width, width), width)


def places(group, narrow):
    me, t = lax.axis_index("sp"), lax.axis_index("tp")
    near = t + 1 - 2 * lax.rem(t, 2)
    far = lax.rem(t + narrow // 2, narrow)
    return me, t, near, far, lax.rem(near + narrow // 2, narrow)


def spread(pairs):
    return sorted(range(1, pairs), key=lambda o: abs(2 * o - pairs))


def around(me, group, sign):
    pairs = group // 2
    half, parity = me // 2, lax.rem(me, 2)
    across = [
        2 * lax.rem(half + pairs + sign * o, pairs) + (parity if side == 0 else 1 - parity)
        for o in spread(pairs)
        for side in range(2)
    ]
    return 2 * half + 1 - parity, across


def remote(src, dst, send, recv, sp, tp):
    return pltpu.make_async_remote_copy(
        src_ref=src, dst_ref=dst, send_sem=send, recv_sem=recv, device_id=(sp, tp), device_id_type=MESH
    )


def meet(peers):
    barrier = pltpu.get_barrier_semaphore()
    for sp, tp in peers:
        pl.semaphore_signal(barrier, inc=1, device_id=(sp, tp), device_id_type=MESH)
    pl.semaphore_wait(barrier, len(peers))


def dots(lhs, rhs, left, right):
    return lax.dot_general(lhs, rhs, (((left,), (right,)), ((), ())), preferred_element_type=jnp.float32)


small_loads = ("ids", "weight", "cot", "conv", "gain")


def whole_kernel(group, narrow, cap, inputs, results, names, *refs):
    r = dict(zip(names, refs[inputs + results :]))
    r["result"] = refs[inputs : inputs + results]
    ids_ref, weight_ref, cot_ref, conv_ref, gain_ref = (r[n] for n in small_loads)
    in_ref, pair_w, down_ref, w_ref, taps_ref = r["in"], r["pair_w"], r["down"], r["proj"], r["taps"]
    out_ref, cot_rows, act_ref, delta, part = r["out"], r["cot_rows"], r["act"], r["delta"], r["part"]
    up_slope, gate_slope, pair_buf = r["up_slope"], r["gate_slope"], r["pair_buf"]
    far_out, far_in, done, home = r["far_out"], r["far_in"], r["done"], r["home"]
    stat_ref, stats_ref, term_ref, terms_ref = r["stat"], r["stats"], r["term"], r["terms"]
    mix_full, parts, pair_in, pair_sum = r["mix_full"], r["parts"], r["pair_in"], r["pair_sum"]
    others, own_sum, extended, beyond = r["others"], r["own_sum"], r["extended"], r["beyond"]
    conv_act, hat_ref, slope_ref, dev_ref = r["conv_act"], r["hat"], r["slope"], r["dev"]
    a_s, a_r, n_s, n_r, f_s, f_r, m_s, m_r = (r[n] for n in ("a_s", "a_r", "n_s", "n_r", "f_s", "f_r", "m_s", "m_r"))
    pn_s, pn_r, pf_s, pf_r, h_s, h_r = (r[n] for n in ("pn_s", "pn_r", "pf_s", "pf_r", "h_s", "h_r"))
    t_s, t_r, u_s, u_r, l_s, o_s = (r[n] for n in ("t_s", "t_r", "u_s", "u_r", "l_s", "o_s"))
    wn_s, wn_r, wf_s, wf_r, wm_s, wm_r = (r[n] for n in ("wn_s", "wn_r", "wf_s", "wf_r", "wm_s", "wm_r"))
    x_s, x_r, z_s, z_r, e_s, e_r = (r[n] for n in ("x_s", "x_r", "z_s", "z_r", "e_s", "e_r"))
    f32, bf16 = jnp.float32, jnp.bfloat16
    me, t, near, far, cross = places(group, narrow)
    partner, across = around(me, group, 1)
    arriving = around(me, group, -1)[1]
    sp_peers = [partner] + across
    peers = [(p, t) for p in sp_peers] + [(me, near), (me, far), (me, cross)]
    barrier = pltpu.get_barrier_semaphore()
    for sp, tp in peers:
        pl.semaphore_signal(barrier, inc=1, device_id=(sp, tp), device_id_type=MESH)

    tokens, width = cot_ref.shape
    slots, model = cot_rows.shape
    hidden = down_ref.shape[0]
    chosen = ids_ref.shape[0]
    channels = width * narrow
    targets = [ids_ref, weight_ref, cot_ref, conv_ref, gain_ref, in_ref]
    targets += [pair_w.at[:, pl.ds(0, hidden)], pair_w.at[:, pl.ds(hidden, hidden)], down_ref]
    targets += [w_ref, taps_ref, r["value"], r["gate"]]
    loads = [pltpu.make_async_copy(refs[k], d, l_s.at[k]) for k, d in enumerate(targets)]
    for c in loads:
        c.start()
    for c in loads[:3]:
        c.wait()

    ids_rows = ids_ref[...]
    lane = lax.broadcasted_iota(jnp.int32, (tokens, 128), 1)
    row = lax.broadcasted_iota(jnp.int32, (8, tokens), 0)
    weight_rows = jnp.zeros((8, tokens), f32)
    for k in range(chosen):
        weight_rows = jnp.where(row == k, weight_ref[k : k + 1, :], weight_rows)
    weights = jnp.transpose(weight_rows)
    experts = -(-group // 8) * 8
    expert = lax.broadcasted_iota(jnp.int32, (experts, tokens), 0)
    hots = [ids_rows[k : k + 1] == expert for k in range(chosen)]
    hot = functools.reduce(jnp.logical_or, hots).astype(f32).astype(bf16)
    first = lax.broadcasted_iota(jnp.int32, (tokens, tokens), 0)
    second = lax.broadcasted_iota(jnp.int32, (tokens, tokens), 1)
    earlier = dots(hot, (first < second).astype(f32).astype(bf16), 1, 0)
    slot_row = lax.broadcasted_iota(jnp.int32, (slots, tokens), 0)
    picks = []
    outgoing = jnp.zeros((slots, width), f32)
    for k in range(chosen):
        slot = jnp.sum(jnp.where(hots[k], earlier, 0.0), axis=0, keepdims=True).astype(jnp.int32)
        dest = ids_rows[k : k + 1] * cap + slot
        pick = (slot_row == dest).astype(f32).astype(bf16)
        scaled = (weights[:, k : k + 1] * cot_ref[...].astype(f32)).astype(bf16)
        outgoing = outgoing + dots(pick, scaled, 1, 0)
        picks.append(pick)
    out_ref[...] = outgoing.astype(bf16)
    pick_any = functools.reduce(jnp.add, picks)

    def block(s):
        return pl.ds(pl.multiple_of(s * cap, cap), cap)

    def spot(s, column):
        return cot_rows.at[block(s), lanes(column, width)]

    cot_rows[block(me), lanes(t, width)] = out_ref[block(me), :]
    pl.semaphore_wait(barrier, len(peers))

    def swap(s):
        return remote(out_ref.at[block(s)], spot(me, t), a_s.at[s], a_r.at[me], s, t)

    def to_far(s):
        return remote(spot(s, t), spot(s, t), f_s.at[s], f_r.at[s], me, far)

    def to_near(s):
        return remote(spot(s, t), spot(s, t), n_s.at[s], n_r.at[s], me, near)

    def onward(s):
        return remote(spot(s, far), spot(s, far), m_s.at[s], m_r.at[s], me, near)

    def part_near(s, k):
        column = near if k == 0 else cross
        return remote(
            part.at[block(s), lanes(column, width)],
            pair_buf.at[k, block(s)],
            pn_s.at[s, k],
            pn_r.at[s, k],
            me,
            near,
        )

    def part_far(s):
        return remote(far_out.at[block(s)], far_in.at[block(s)], pf_s.at[s], pf_r.at[s], me, far)

    def to_home(s):
        return remote(done.at[block(s)], home.at[block(me)], h_s.at[s], h_r.at[me], s, t)

    def from_home(s):
        return remote(done.at[block(s)], home.at[block(s)], h_s.at[s], h_r.at[s], s, t)

    def arrive(s):
        remote(out_ref.at[block(s)], spot(s, t), a_s.at[s], a_r.at[s], s, t).wait_recv()

    def fan(s):
        to_far(s).start()
        to_near(s).start()

    def relay(s):
        to_far(s).wait_recv()
        onward(s).start()

    def slopes(piece, pieces):
        count = slots // pieces
        span = pl.ds(piece * count, count)
        both = jnp.dot(in_ref[span, :], pair_w[...], preferred_element_type=f32)
        gate_lin, up_lin = both[:, :hidden], both[:, hidden:]
        gate_c = jnp.minimum(gate_lin, clamp_limit)
        up_c = jnp.clip(up_lin, -clamp_limit, clamp_limit)
        sigma = jax.nn.sigmoid(swish_alpha * gate_c)
        lift, gated = up_c + 1.0, gate_c * sigma
        act_ref[span, :] = (lift * gated).astype(bf16)
        up_open = (up_lin > -clamp_limit) & (up_lin < clamp_limit)
        up_slope[span, :] = jnp.where(up_open, gated, 0.0)
        slope = lift * (sigma + swish_alpha * gated * (1.0 - sigma))
        gate_slope[span, :] = jnp.where(gate_lin < clamp_limit, slope, 0.0)

    def compute(s, ready):
        rows = block(s)
        if not ready:
            remote(spot(s, near), spot(s, near), n_s.at[s], n_r.at[s], me, near).wait_recv()
            remote(spot(s, cross), spot(s, cross), m_s.at[s], m_r.at[s], me, near).wait_recv()
        d_act = dots(cot_rows[rows, :], down_ref[...], 1, 1)
        d_gate = (d_act * gate_slope[rows, :]).astype(bf16)
        d_up = (d_act * up_slope[rows, :]).astype(bf16)
        delta[rows, pl.ds(0, hidden)] = d_gate
        delta[rows, pl.ds(hidden, hidden)] = d_up
        cut = min(model, 1024)
        for j in range(model // cut):
            span = pl.ds(j * cut, cut)
            part[rows, span] = dots(delta[rows, :], pair_w[span, :], 1, 1).astype(bf16)
        part_near(s, 1).start()
        part_near(s, 0).start()

    def pair_up(s):
        rows = block(s)
        part_near(s, 1).wait_recv()
        pair = part[rows, lanes(far, width)].astype(f32) + pair_buf[1, rows].astype(f32)
        far_out[rows, :] = pair.astype(bf16)
        part_far(s).start()

    def finish(s, own):
        rows = block(s)
        part_near(s, 0).wait_recv()
        part_far(s).wait_recv()
        total = part[rows, lanes(t, width)].astype(f32)
        total = total + pair_buf[0, rows].astype(f32) + far_in[rows, :].astype(f32)
        if own:
            home[rows, :] = total.astype(bf16)
        else:
            done[rows, :] = total.astype(bf16)
            to_home(s).start()

    for s in across + [partner]:
        swap(s).start()
    fan(me)
    loads[3].wait()
    conv = conv_ref[...].astype(f32)
    sums = jnp.where(lane == 0, jnp.sum(conv, axis=1, keepdims=True), 0.0)
    sums = jnp.where(lane == 1, jnp.sum(conv * conv, axis=1, keepdims=True), sums)
    stat_ref[...] = jnp.transpose(sums)[:8]
    small = []
    for k, p in enumerate((near, far, cross)):
        c = remote(stat_ref, stats_ref.at[t], t_s.at[k], t_r.at[k], me, p)
        c.start()
        small.append(c)
    stats_ref[t] = stat_ref[...]
    for c in loads[4:9]:
        c.wait()
    pieces = 4
    slopes(0, pieces)
    arrive(partner)
    fan(partner)
    relay(me)
    fill = [functools.partial(slopes, p, pieces) for p in range(1, pieces)]
    count = len(arriving)

    def at(k):
        return arriving[k]

    def normalize():
        for c in small:
            c.wait_recv()
        total = functools.reduce(jnp.add, [stats_ref[k] for k in range(narrow)])
        total = jnp.transpose(total)
        mean = total[:, 0:1] / channels
        var = total[:, 1:2] / channels - mean * mean
        inverse = lax.rsqrt(var + norm_epsilon)
        hat = (conv_ref[...].astype(f32) - mean) * inverse
        normed = hat * gain_ref[...]
        sigma = jax.nn.sigmoid(normed)
        dev_ref[...] = inverse
        hat_ref[...] = hat
        conv_act[...] = (normed * sigma).astype(bf16)
        slope_ref[...] = sigma * (1.0 + normed * (1.0 - sigma)) * gain_ref[...]

    outs = [r["gate_stage"], r["up_stage"], r["down_stage"], own_sum, r["value_stage"], r["grad_stage"]]
    stores = [pltpu.make_async_copy(d, r["result"][k], o_s.at[k]) for k, d in enumerate(outs)]
    for i in range(count + 5):
        if i - 5 >= 0 and i - 5 < count:
            finish(at(i - 5), False)
        if 0 <= i - 3 < count:
            pair_up(at(i - 3))
        if 0 <= i - 2 < count:
            compute(at(i - 2), False)
        if i < count:
            arrive(at(i))
            fan(at(i))
        if i == 0:
            relay(partner)
        elif i - 1 < count:
            relay(at(i - 1))
        for _ in range(2 - i):
            fill.pop(0)()
        if i == min(3, count):
            normalize()
        if i == count:
            compute(partner, False)
            compute(me, False)
        if i == count + 2:
            pair_up(partner)
            pair_up(me)
            outs[2][...] = dots(act_ref[...], cot_rows[...], 0, 0).astype(bf16)
            stores[2].start()
        if i == count + 3:
            outs[0][...] = dots(in_ref[...], delta[:, :hidden], 0, 0).astype(bf16)
            stores[0].start()
        if i == count + 4:
            outs[1][...] = dots(in_ref[...], delta[:, hidden:], 0, 0).astype(bf16)
            stores[1].start()
    finish(partner, False)
    finish(me, True)
    for s in sp_peers:
        from_home(s).wait_recv()
    summed = dots(pick_any, home[...], 0, 0)
    mix_full[:, lanes(t, width)] = (cot_ref[...].astype(f32) + summed).astype(bf16)

    pieces = 2
    piece_rows = tokens // pieces

    def wide(k, column):
        return mix_full.at[pl.ds(k * piece_rows, piece_rows), lanes(column, width)]

    def wide_far(k):
        return remote(wide(k, t), wide(k, t), wf_s.at[k], wf_r.at[k], me, far)

    def wide_near(k):
        return remote(wide(k, t), wide(k, t), wn_s.at[k], wn_r.at[k], me, near)

    def wide_on(k):
        return remote(wide(k, far), wide(k, far), wm_s.at[k], wm_r.at[k], me, near)

    pairs = group // 2
    parity = lax.rem(me, 2)
    half = me // 2
    ahead, behind = lax.rem(me + 1, group), lax.rem(me + group - 1, group)
    alike = [lax.rem(half + o, pairs) for o in spread(pairs)]
    order = alike + [half]
    columns = [t, near, far, cross]
    sub = parts.shape[1]

    def pair_swap(q, c):
        side = lanes(columns[c], width)
        return remote(
            parts.at[2 * q + 1 - parity, :, side],
            pair_in.at[q, :, side],
            x_s.at[q, c],
            x_r.at[q, c],
            partner,
            t,
        )

    def slot_of(source, target):
        return lax.rem(target - source + pairs, pairs) - 1

    def passing(source, target, c):
        return others.at[slot_of(source, target), :, lanes(columns[c], width)], z_r.at[source, c]

    def scatter(q, c):
        slot, arrival = passing(half, q, c)
        source = pair_sum.at[q, :, lanes(columns[c], width)]
        return remote(source, slot, z_s.at[q, c], arrival, 2 * q + parity, t)

    def project(c):
        side = lanes(columns[c], width)
        product = dots(conv_act[...], mix_full[:, side], 0, 0)
        parts[:, :, side] = product.reshape(group, sub, width).astype(bf16)
        for q in order:
            pair_swap(q, c).start()

    def absorb(q, c, own):
        side = lanes(columns[c], width)
        pair_swap(q, c).wait_recv()
        both = parts[2 * q + parity, :, side].astype(f32) + pair_in[q, :, side].astype(f32)
        if own:
            own_sum[:, side] = both
        else:
            pair_sum[q, :, side] = both.astype(bf16)
            scatter(q, c).start()

    tasks = [functools.partial(absorb, q, c, k == pairs - 1) for c in range(narrow) for k, q in enumerate(order)]

    def run(number):
        for _ in range(min(number, len(tasks))):
            tasks.pop(0)()

    for k in range(pieces):
        wide_far(k).start()
    for k in range(pieces):
        wide_near(k).start()
    project(0)
    for k in range(pieces):
        wide_near(k).wait_recv()
    project(1)
    for k in range(pieces):
        wide_far(k).wait_recv()
        wide_on(k).start()
    run(pairs // 2)
    loads[9].wait()
    project(2)
    run(pairs // 2)
    for k in range(pieces):
        wide_on(k).wait_recv()
    ng = dots(mix_full[...], w_ref[...], 1, 1) * slope_ref[...]
    hat = hat_ref[...]
    sums = jnp.where(lane == 0, jnp.sum(ng, axis=1, keepdims=True), 0.0)
    sums = jnp.where(lane == 1, jnp.sum(ng * hat, axis=1, keepdims=True), sums)
    term_ref[...] = jnp.transpose(sums)[:8]
    terms = []
    for k, p in enumerate((near, far, cross)):
        terms.append(remote(term_ref, terms_ref.at[k], u_s.at[k], u_r.at[k], me, p))
        terms[k].start()
    run(pairs // 2)
    total = term_ref[...]
    for k, c in enumerate(terms):
        c.wait_recv()
        total = total + terms_ref[k]
    total = jnp.transpose(total)
    first, second = total[:, 0:1] / channels, total[:, 1:2] / channels
    extended[pl.ds(0, tokens), :] = dev_ref[...] * (ng - first - hat * second)
    halo = beyond.shape[0]
    halo_send = remote(extended.at[pl.ds(0, halo)], beyond, e_s.at[0], e_r.at[0], behind, t)
    halo_send.start()
    project(3)
    for c in loads[10:]:
        c.wait()

    reach = taps_ref.shape[0]
    step = 32
    strips = width // 128

    def convolve(index, carry):
        start = pl.multiple_of((index // strips) * step, step)
        column = lanes(lax.rem(index, strips), 128)
        total = jnp.zeros((step, 128), f32)
        window = extended[pl.ds(start, step + halo), column]
        for turn in range(8):
            shifted = window if turn == 0 else pltpu.roll(window, step + halo - turn, 0)
            for j in range(turn, reach, 8):
                total = total + taps_ref[reach - 1 - j : reach - j, column] * shifted[j - turn : j - turn + step]
        here = pl.ds(start, step)
        gate_sig = jax.nn.sigmoid(r["gate"][here, column].astype(f32))
        moved = total * gate_sig
        outs[4][here, column] = moved.astype(bf16)
        outs[5][here, column] = (moved * r["value"][here, column].astype(f32) * (1.0 - gate_sig)).astype(bf16)
        return carry

    turns = (tokens // step - 1) * strips
    rest = len(tasks) - 2
    marks = [turns * i // rest for i in range(rest + 1)]
    for i in range(rest):
        run(1)
        lax.fori_loop(marks[i], marks[i + 1], convolve, 0)
    run(1)
    halo_send.wait_recv()
    tail_rows = beyond[...]
    extended[pl.ds(tokens, halo), :] = jnp.where(me == group - 1, jnp.zeros_like(tail_rows), tail_rows)
    lax.fori_loop(turns, turns + strips, convolve, 0)
    stores[4].start()
    stores[5].start()
    run(1)
    for c in range(narrow):
        side = lanes(columns[c], width)
        total = own_sum[:, side]
        for q in alike:
            slot, arrival = passing(q, half, c)
            remote(pair_sum.at[q, :, side], slot, z_s.at[q, c], arrival, 2 * q + parity, t).wait_recv()
            total = total + others[slot_of(q, half), :, side].astype(f32)
        own_sum[:, side] = total
    stores[3].start()
    for s in [me] + sp_peers:
        to_far(s).wait_send()
        to_near(s).wait_send()
        onward(s).wait_send()
        part_near(s, 0).wait_send()
        part_near(s, 1).wait_send()
        part_far(s).wait_send()
    for s in sp_peers:
        swap(s).wait_send()
        to_home(s).wait_send()
    for c in small + terms:
        c.wait_send()
    for k in range(pieces):
        wide_far(k).wait_send()
        wide_near(k).wait_send()
        wide_on(k).wait_send()
    halo_send.wait_send()
    for c in range(narrow):
        for q in order:
            pair_swap(q, c).wait_send()
        for q in alike:
            scatter(q, c).wait_send()
    for c in stores:
        c.wait()


def whole_pass(*args):
    group, narrow = lax.axis_size("sp"), lax.axis_size("tp")
    ids, weight, cot, conv, gain, rows_in, gate_w, up_w, down_w, proj_w, taps, value, gate = args
    tokens, width = cot.shape
    slots, model = rows_in.shape
    hidden = down_w.shape[0]
    cap = slots // group
    pairs = group // 2
    sub = width // group
    halo = -(-(taps.shape[0] - 1) // 8) * 8
    f32, bf16 = jnp.float32, jnp.bfloat16
    dma = pltpu.SemaphoreType.DMA
    rows = (slots, width)
    tile = (tokens, width)
    results = [
        ((model, hidden), bf16),
        ((model, hidden), bf16),
        ((hidden, model), bf16),
        ((sub, model), f32),
        (tile, bf16),
        (tile, bf16),
    ]
    scratch = dict(
        ids=VMEM(ids.shape, ids.dtype),
        weight=VMEM(weight.shape, weight.dtype),
        cot=VMEM(tile, bf16),
        conv=VMEM(tile, bf16),
        gain=VMEM(gain.shape, f32),
        pair_w=VMEM((model, 2 * hidden), bf16),
        down=VMEM(down_w.shape, bf16),
        proj=VMEM(proj_w.shape, bf16),
        taps=VMEM(taps.shape, f32),
        value=VMEM(tile, bf16),
        gate=VMEM(tile, bf16),
        out=VMEM(rows, bf16),
        cot_rows=VMEM((slots, model), bf16),
        act=VMEM((slots, hidden), bf16),
        up_slope=VMEM((slots, hidden), f32),
        gate_slope=VMEM((slots, hidden), f32),
        delta=VMEM((slots, 2 * hidden), bf16),
        part=VMEM((slots, model), bf16),
        pair_buf=VMEM((2,) + rows, bf16),
        far_out=VMEM(rows, bf16),
        far_in=VMEM(rows, bf16),
        done=VMEM(rows, bf16),
        home=VMEM(rows, bf16),
        stat=VMEM((8, tokens), f32),
        stats=VMEM((narrow, 8, tokens), f32),
        term=VMEM((8, tokens), f32),
        terms=VMEM((narrow - 1, 8, tokens), f32),
        mix_full=VMEM((tokens, model), bf16),
        parts=VMEM((group, sub, model), bf16),
        pair_in=VMEM((pairs, sub, model), bf16),
        pair_sum=VMEM((pairs, sub, model), bf16),
        others=VMEM((pairs - 1, sub, model), bf16),
        own_sum=VMEM((sub, model), f32),
        extended=VMEM((tokens + halo, width), f32),
        beyond=VMEM((halo, width), f32),
        conv_act=VMEM(tile, bf16),
        hat=VMEM(tile, f32),
        slope=VMEM(tile, f32),
        dev=VMEM((tokens, 1), f32),
        gate_stage=VMEM((model, hidden), bf16),
        up_stage=VMEM((model, hidden), bf16),
        down_stage=VMEM((hidden, model), bf16),
        value_stage=VMEM(tile, bf16),
        grad_stage=VMEM(tile, bf16),
        l_s=dma((len(args),)),
        o_s=dma((len(results),)),
        e_s=dma((1,)),
        e_r=dma((1,)),
    )
    scratch["in"] = VMEM(rows_in.shape, bf16)
    for n in ("a", "n", "f", "m", "pf", "h"):
        scratch[n + "_s"] = scratch[n + "_r"] = dma((group,))
    scratch["pn_s"] = scratch["pn_r"] = dma((group, 2))
    for n in ("t", "u"):
        scratch[n + "_s"] = scratch[n + "_r"] = dma((narrow - 1,))
    for n in ("wn", "wf", "wm"):
        scratch[n + "_s"] = scratch[n + "_r"] = dma((2,))
    for n in ("x", "z"):
        scratch[n + "_s"] = scratch[n + "_r"] = dma((pairs, narrow))

    def body(*refs):
        whole_kernel(group, narrow, cap, len(args), len(results), tuple(scratch), *refs)

    return pl.pallas_call(
        body,
        name="whole_kernel",
        out_shape=tuple(jax.ShapeDtypeStruct(*x) for x in results),
        in_specs=[pl.BlockSpec(memory_space=pl.ANY)] * len(args),
        out_specs=[pl.BlockSpec(memory_space=pl.ANY)] * len(results),
        scratch_shapes=list(scratch.values()),
        compiler_params=pltpu.CompilerParams(
            collective_id=0, has_side_effects=True, vmem_limit_bytes=60 * 1024 * 1024
        ),
    )(*args)


def per_device(
    cot_out,
    route_ids,
    route_weight,
    expert_inputs,
    w_gate,
    w_up,
    w_down,
    w_proj,
    conv_out,
    channel_norm_gain,
    taps,
    value_pre,
    gate_pre,
):
    group_size = lax.axis_size("sp")
    rows_in = expert_inputs[0]
    slot_rows, model_width = rows_in.shape
    capacity = slot_rows // group_size
    fitted = -(-capacity // 16) * 16
    if fitted != capacity:
        rows_in = rows_in.reshape(group_size, capacity, model_width)
        rows_in = jnp.pad(rows_in, ((0, 0), (0, fitted - capacity), (0, 0)))
        rows_in = rows_in.reshape(group_size * fitted, model_width)
    grad_gate_part, grad_up_part, grad_down, grad_proj, grad_value, grad_gate = whole_pass(
        route_ids.T,
        route_weight.T,
        cot_out,
        conv_out,
        channel_norm_gain[None, :],
        rows_in,
        w_gate[0],
        w_up[0],
        w_down[0],
        w_proj,
        taps,
        value_pre,
        gate_pre,
    )
    return (
        grad_gate_part[None],
        grad_up_part[None],
        grad_down[None],
        grad_proj,
        grad_value,
        grad_gate,
    )


def solution(mesh):
    return jax.shard_map(
        per_device,
        mesh=mesh,
        in_specs=(
            P("sp", "tp"),
            P("sp", None),
            P("sp", None),
            P("sp", None, None),
            P("sp", None, "tp"),
            P("sp", None, "tp"),
            P("sp", "tp", None),
            P("tp", None),
            P("sp", "tp"),
            P("tp"),
            P(None, "tp"),
            P("sp", "tp"),
            P("sp", "tp"),
        ),
        out_specs=(
            P("sp", None, "tp"),
            P("sp", None, "tp"),
            P("sp", "tp", None),
            P(("tp", "sp"), None),
            P("sp", "tp"),
            P("sp", "tp"),
        ),
        check_vma=False,
    )
```

time: 130 us -> 99.4 us (0.76)
  Pallas kernels: 111 us -> 90.7 us
  other arithmetic: 5.73 us -> 0 us
  matrix products: 5.37 us -> 0 us
  local copies, waits for them, and re-layouts: 6.06 us -> 7.88 us
    pallas_call x3 -> x1, Pallas kernels: 111 us -> 90.7 us  [whole_pass(): pl.pallas_call(body, name='whole_kernel', out_shape=tuple((jax.ShapeDtype...]
    dot_general x2 -> x0, matrix products: 5.37 us -> none  [the longest x1 3.09 us: per_device(): d_act_conv = jnp.dot(mix_full, w_proj.T, preferred_element_type=f32)]
    reduce_sum x2 -> x0, other arithmetic: 2.21 us -> none  [the longest x1 1.44 us: per_device(): grad_proj = own_proj + jnp.sum(other_proj.astype(f32), axis=0)]
    add x1 -> x0, other arithmetic: 1.89 us -> none  [per_device(): grad_proj = own_proj + jnp.sum(other_proj.astype(f32), axis=0)]
    unnamed x25 -> x14, local copies, waits for them, and re-layouts: 6.06 us -> 7.88 us
where the time goes in v2:
time: 99.4 us; the launch traced here: 99.3 us
  Pallas kernels  90.7 us (91%)
  local copies, waits for them, and re-layouts  7.88 us (8%)
    pallas_call x1, Pallas kernels, whole_pass(): pl.pallas_call(body, name='whole_kernel', out_shape=tuple((jax.ShapeDtype...  90.7 us
    unnamed x14, local copies, waits for them, and re-layouts  7.88 us

profile of v2, /device:TPU:0, one launch (start us, length us, event | category | flops | bytes accessed | tf_op | source)
XLA Modules:
  0.0 99.3 jit_solution(18071056900091041565)
XLA Ops:
  0.6 90.7 %whole_kernel.1 = (bf16[2048,256]{1,0:T(8,128)(2,1)}, bf16[2048,256]{1,0:T(8,128)(2,1)}, bf16[256,2048]{1,0:T(8,128)(2,1)}, f32[64,2048]{1,0:T(8,128)}, bf16[256...) custom-call(s32[2,256]{1,0:T(2,128)} %bitcast.17, f32[2,256]{1,0:T(2,128)} %bitcast.18, bf16[256,512]{1,0:T(8,128)(2,1)} %refs_2_.1, ...), custom_call_target="tpu_custom_call" | custom-call | tf_op jit(solution)/shard_map/whole_kernel/pallas_call | solution.py:583
  91.4 0.0 copy-start
  91.4 0.0 copy-start.1
  91.4 2.4 %copy.25 = bf16[1,2048,256]{2,1,0:T(8,128)(2,1)} copy(bf16[1,2048,256]{2,1,0:T(8,128)(2,1)} %bitcast.16) | data formatting | bytes 2097152
  93.8 0.0 copy-start.3
  93.8 0.0 copy-start.2
  93.8 2.3 %copy.26 = bf16[1,2048,256]{2,1,0:T(8,128)(2,1)} copy(bf16[1,2048,256]{2,1,0:T(8,128)(2,1)} %bitcast.15) | data formatting | bytes 2097152
  96.1 0.0 copy-done
  96.1 1.0 copy.27
  97.1 0.0 copy-done.1
  97.1 0.8 copy.28
  97.9 0.0 copy-done.3
  97.9 0.7 copy.29
  98.6 0.0 copy-done.2
  98.6 0.7 copy.30
Async XLA Ops:
  91.4 4.7 %copy-start = (bf16[256,2048]{1,0:T(8,128)(2,1)S(1)}, bf16[256,2048]{1,0:T(8,128)(2,1)}, u32[]{:S(2)}) copy-start(bf16[256,2048]{1,0:T(8,128)(2,1)} %get-tuple-element.14) | copy-start | bytes 3145732
  91.4 5.7 %copy-start.1 = (f32[64,2048]{1,0:T(8,128)S(1)}, f32[64,2048]{1,0:T(8,128)}, u32[]{:S(2)}) copy-start(f32[64,2048]{1,0:T(8,128)} %get-tuple-element.27) | copy-start | bytes 1572868
  93.8 4.1 %copy-start.3 = (bf16[256,512]{1,0:T(8,128)(2,1)S(1)}, bf16[256,512]{1,0:T(8,128)(2,1)}, u32[]{:S(2)}) copy-start(bf16[256,512]{1,0:T(8,128)(2,1)} %get-tuple-element.28) | copy-start | bytes 786436
  93.8 4.8 %copy-start.2 = (bf16[256,512]{1,0:T(8,128)(2,1)S(1)}, bf16[256,512]{1,0:T(8,128)(2,1)}, u32[]{:S(2)}) copy-start(bf16[256,512]{1,0:T(8,128)(2,1)} %get-tuple-element.29) | copy-start | bytes 786436

commit v3 on v2

--- a/solution.py
+++ b/solution.py
@@ -29,14 +29,23 @@
     return sorted(range(1, pairs), key=lambda o: abs(2 * o - pairs))
 
 
-def around(me, group, sign):
-    pairs = group // 2
+def nearest(here, count):
+    def reaches(a, b):
+        return (a - b + count) // count
+
+    upper = reaches(here, count - 1 - here)
+    inner = here + (count - 1 - 2 * here) * upper
+    found = []
+    for k in range(count - 1):
+        lone = reaches(k, 2 * inner)
+        both = k // 2 + 1 if k % 2 == 0 else -(k // 2 + 1)
+        found.append(here + (1 - lone) * both + lone * (1 - 2 * upper) * (k - inner + 1))
+    return found
+
+
+def around(me, group):
     half, parity = me // 2, lax.rem(me, 2)
-    across = [
-        2 * lax.rem(half + pairs + sign * o, pairs) + (parity if side == 0 else 1 - parity)
-        for o in spread(pairs)
-        for side in range(2)
-    ]
+    across = [2 * z + side for z in nearest(half, group // 2) for side in (parity, 1 - parity)]
     return 2 * half + 1 - parity, across
 
 
@@ -79,8 +88,8 @@
     x_s, x_r, z_s, z_r, e_s, e_r = (r[n] for n in ("x_s", "x_r", "z_s", "z_r", "e_s", "e_r"))
     f32, bf16 = jnp.float32, jnp.bfloat16
     me, t, near, far, cross = places(group, narrow)
-    partner, across = around(me, group, 1)
-    arriving = around(me, group, -1)[1]
+    partner, across = around(me, group)
+    arriving = across
     sp_peers = [partner] + across
     peers = [(p, t) for p in sp_peers] + [(me, near), (me, far), (me, cross)]
     barrier = pltpu.get_barrier_semaphore()
@@ -584,13 +593,34 @@
         body,
         name="whole_kernel",
         out_shape=tuple(jax.ShapeDtypeStruct(*x) for x in results),
-        in_specs=[pl.BlockSpec(memory_space=pl.ANY)] * len(args),
+        in_specs=[pl.BlockSpec(memory_space=pltpu.HBM)] * len(args),
         out_specs=[pl.BlockSpec(memory_space=pl.ANY)] * len(results),
         scratch_shapes=list(scratch.values()),
         compiler_params=pltpu.CompilerParams(
-            collective_id=0, has_side_effects=True, vmem_limit_bytes=60 * 1024 * 1024
+            collective_id=0, has_side_effects=True, vmem_limit_bytes=48 * 1024 * 1024
         ),
-    )(*args)
+    )(*[pltpu.with_memory_space_constraint(x, pltpu.HBM) for x in args])
+
+
+def emit_kernel(count, *refs):
+    sems = refs[-1]
+    copies = [pltpu.make_async_copy(refs[k], refs[count + k], sems.at[k]) for k in range(count)]
+    for c in copies:
+        c.start()
+    for c in copies:
+        c.wait()
+
+
+def emit(*results):
+    return pl.pallas_call(
+        functools.partial(emit_kernel, len(results)),
+        name="emit",
+        out_shape=tuple(jax.ShapeDtypeStruct(x.shape, x.dtype) for x in results),
+        in_specs=[pl.BlockSpec(memory_space=pl.ANY)] * len(results),
+        out_specs=[pl.BlockSpec(memory_space=pltpu.HBM)] * len(results),
+        scratch_shapes=[pltpu.SemaphoreType.DMA((len(results),))],
+        compiler_params=pltpu.CompilerParams(vmem_limit_bytes=1024 * 1024),
+    )(*results)
 
 
 def per_device(
@@ -617,7 +647,8 @@
         rows_in = rows_in.reshape(group_size, capacity, model_width)
         rows_in = jnp.pad(rows_in, ((0, 0), (0, fitted - capacity), (0, 0)))
         rows_in = rows_in.reshape(group_size * fitted, model_width)
-    grad_gate_part, grad_up_part, grad_down, grad_proj, grad_value, grad_gate = whole_pass(
+    grad_gate_part, grad_up_part, grad_down, grad_proj, grad_value, grad_gate = emit(
+        *whole_pass(
         route_ids.T,
         route_weight.T,
         cot_out,
@@ -631,6 +662,7 @@
         taps,
         value_pre,
         gate_pre,
+        )
     )
     return (
         grad_gate_part[None],

time: 99.4 us -> 93.7 us (0.943)
  local copies, waits for them, and re-layouts: 7.88 us -> 0 us
  Pallas kernels: 90.7 us -> 92.5 us
    unnamed x14 -> x0, local copies, waits for them, and re-layouts: 7.88 us -> none
    pallas_call x0 -> x1, Pallas kernels: none -> 2.05 us  [emit(): pl.pallas_call(functools.partial(emit_kernel, len(results)), name='emit',...]
where the time goes in v3:
time: 93.7 us; the launch traced here: 93.3 us
  Pallas kernels  92.5 us (99%)
    pallas_call x1, Pallas kernels, whole_pass(): pl.pallas_call(body, name='whole_kernel', out_shape=tuple((jax.ShapeDtype...  90.4 us
    pallas_call x1, Pallas kernels, emit(): pl.pallas_call(functools.partial(emit_kernel, len(results)), name='emit',...  2.05 us

profile of v3, /device:TPU:0, one launch (start us, length us, event | category | flops | bytes accessed | tf_op | source)
XLA Modules:
  0.0 93.3 jit_solution(3460578342062589126)
XLA Ops:
  0.6 90.4 %whole_kernel.1 = (bf16[2048,256]{1,0:T(8,128)(2,1)S(1)}, bf16[2048,256]{1,0:T(8,128)(2,1)S(1)}, bf16[256,2048]{1,0:T(8,128)(2,1)S(1)}, f32[64,2048]{1,0:T(8,128...) custom-call(s32[2,256]{1,0:T(2,128)} %bitcast.14, f32[2,256]{1,0:T(2,128)} %bitcast.15, ...), custom_call_target="tpu_custom_call" | custom-call | tf_op jit(solution)/shard_map/whole_kernel/pallas_call | solution.py:592
  91.0 2.1 %emit.1 = (bf16[2048,256]{1,0:T(8,128)(2,1)}, bf16[2048,256]{1,0:T(8,128)(2,1)}, bf16[256,2048]{1,0:T(8,128)(2,1)}, f32[64,2048]{1,0:T(8,128)}, bf16[256,512]{1,0:T(8,128)(2,1)}, /*index=5*/bf16[256,512]{1,0:T(8,128)(2,1)}) custom-call(bf16[2048,256]{1,0:T(8,128)(2,1)S(1)} %get-tuple-element.18.refs_0_, bf16[2048,256]{1,0:T(8,128)(2,1)S(1)} %get-tuple-element.19.refs_1_, ...), custom_call_target="tpu_custom_call" | custom-call | tf_op jit(solution)/shard_map/emit/pallas_call | solution.py:615

commit v4 on v3

--- a/solution.py
+++ b/solution.py
@@ -78,14 +78,14 @@
     up_slope, gate_slope, pair_buf = r["up_slope"], r["gate_slope"], r["pair_buf"]
     far_out, far_in, done, home = r["far_out"], r["far_in"], r["done"], r["home"]
     stat_ref, stats_ref, term_ref, terms_ref = r["stat"], r["stats"], r["term"], r["terms"]
-    mix_full, parts, pair_in, pair_sum = r["mix_full"], r["parts"], r["pair_in"], r["pair_sum"]
-    others, own_sum, extended, beyond = r["others"], r["own_sum"], r["extended"], r["beyond"]
+    mix_both, product, kept, own_sum = r["mix_both"], r["product"], r["kept"], r["own_sum"]
+    extended, beyond = r["extended"], r["beyond"]
     conv_act, hat_ref, slope_ref, dev_ref = r["conv_act"], r["hat"], r["slope"], r["dev"]
     a_s, a_r, n_s, n_r, f_s, f_r, m_s, m_r = (r[n] for n in ("a_s", "a_r", "n_s", "n_r", "f_s", "f_r", "m_s", "m_r"))
     pn_s, pn_r, pf_s, pf_r, h_s, h_r = (r[n] for n in ("pn_s", "pn_r", "pf_s", "pf_r", "h_s", "h_r"))
     t_s, t_r, u_s, u_r, l_s, o_s = (r[n] for n in ("t_s", "t_r", "u_s", "u_r", "l_s", "o_s"))
     wn_s, wn_r, wf_s, wf_r, wm_s, wm_r = (r[n] for n in ("wn_s", "wn_r", "wf_s", "wf_r", "wm_s", "wm_r"))
-    x_s, x_r, z_s, z_r, e_s, e_r = (r[n] for n in ("x_s", "x_r", "z_s", "z_r", "e_s", "e_r"))
+    x_s, x_r, y_s, y_r, e_s, e_r = (r[n] for n in ("x_s", "x_r", "y_s", "y_r", "e_s", "e_r"))
     f32, bf16 = jnp.float32, jnp.bfloat16
     me, t, near, far, cross = places(group, narrow)
     partner, across = around(me, group)
@@ -158,25 +158,33 @@
     def onward(s):
         return remote(spot(s, far), spot(s, far), m_s.at[s], m_r.at[s], me, near)
 
-    def part_near(s, k):
+    hw = width // 2
+
+    def piece_of(column, h):
+        return pl.ds(pl.multiple_of(column * width + h * hw, hw), hw)
+
+    def part_near(s, k, h):
         column = near if k == 0 else cross
         return remote(
-            part.at[block(s), lanes(column, width)],
-            pair_buf.at[k, block(s)],
-            pn_s.at[s, k],
-            pn_r.at[s, k],
+            part.at[block(s), piece_of(column, h)],
+            pair_buf.at[k, block(s), pl.ds(h * hw, hw)],
+            pn_s.at[s, 2 * k + h],
+            pn_r.at[s, 2 * k + h],
             me,
             near,
         )
 
-    def part_far(s):
-        return remote(far_out.at[block(s)], far_in.at[block(s)], pf_s.at[s], pf_r.at[s], me, far)
-
-    def to_home(s):
-        return remote(done.at[block(s)], home.at[block(me)], h_s.at[s], h_r.at[me], s, t)
-
-    def from_home(s):
-        return remote(done.at[block(s)], home.at[block(s)], h_s.at[s], h_r.at[s], s, t)
+    def part_far(s, h):
+        side = pl.ds(h * hw, hw)
+        return remote(far_out.at[block(s), side], far_in.at[block(s), side], pf_s.at[s, h], pf_r.at[s, h], me, far)
+
+    def to_home(s, h):
+        side = pl.ds(h * hw, hw)
+        return remote(done.at[block(s), side], home.at[block(me), side], h_s.at[s, h], h_r.at[me, h], s, t)
+
+    def from_home(s, h):
+        side = pl.ds(h * hw, hw)
+        return remote(done.at[block(s), side], home.at[block(s), side], h_s.at[s, h], h_r.at[s, h], s, t)
 
     def arrive(s):
         remote(out_ref.at[block(s)], spot(s, t), a_s.at[s], a_r.at[s], s, t).wait_recv()
@@ -209,7 +217,7 @@
         if not ready:
             remote(spot(s, near), spot(s, near), n_s.at[s], n_r.at[s], me, near).wait_recv()
             remote(spot(s, cross), spot(s, cross), m_s.at[s], m_r.at[s], me, near).wait_recv()
-        d_act = dots(cot_rows[rows, :], down_ref[...], 1, 1)
+        d_act = dots(cot_rows[rows, :], r["down_t"][...], 1, 0)
         d_gate = (d_act * gate_slope[rows, :]).astype(bf16)
         d_up = (d_act * up_slope[rows, :]).astype(bf16)
         delta[rows, pl.ds(0, hidden)] = d_gate
@@ -217,28 +225,31 @@
         cut = min(model, 1024)
         for j in range(model // cut):
             span = pl.ds(j * cut, cut)
-            part[rows, span] = dots(delta[rows, :], pair_w[span, :], 1, 1).astype(bf16)
-        part_near(s, 1).start()
-        part_near(s, 0).start()
-
-    def pair_up(s):
+            part[rows, span] = dots(delta[rows, :], r["pair_t"][:, span], 1, 0).astype(bf16)
+        for h in range(2):
+            part_near(s, 1, h).start()
+            part_near(s, 0, h).start()
+
+    def pair_up(s, h):
         rows = block(s)
-        part_near(s, 1).wait_recv()
-        pair = part[rows, lanes(far, width)].astype(f32) + pair_buf[1, rows].astype(f32)
-        far_out[rows, :] = pair.astype(bf16)
-        part_far(s).start()
-
-    def finish(s, own):
+        side = pl.ds(h * hw, hw)
+        part_near(s, 1, h).wait_recv()
+        pair = part[rows, piece_of(far, h)].astype(f32) + pair_buf[1, rows, side].astype(f32)
+        far_out[rows, side] = pair.astype(bf16)
+        part_far(s, h).start()
+
+    def finish(s, h, own):
         rows = block(s)
-        part_near(s, 0).wait_recv()
-        part_far(s).wait_recv()
-        total = part[rows, lanes(t, width)].astype(f32)
-        total = total + pair_buf[0, rows].astype(f32) + far_in[rows, :].astype(f32)
+        side = pl.ds(h * hw, hw)
+        part_near(s, 0, h).wait_recv()
+        part_far(s, h).wait_recv()
+        total = part[rows, piece_of(t, h)].astype(f32)
+        total = total + pair_buf[0, rows, side].astype(f32) + far_in[rows, side].astype(f32)
         if own:
-            home[rows, :] = total.astype(bf16)
+            home[rows, side] = total.astype(bf16)
         else:
-            done[rows, :] = total.astype(bf16)
-            to_home(s).start()
+            done[rows, side] = total.astype(bf16)
+            to_home(s, h).start()
 
     for s in across + [partner]:
         swap(s).start()
@@ -258,14 +269,22 @@
         c.wait()
     pieces = 4
     slopes(0, pieces)
+    slopes(1, pieces)
+    r["down_t"][...] = jnp.transpose(down_ref[...])
+    r["pair_t"][...] = jnp.transpose(pair_w[...])
     arrive(partner)
     fan(partner)
+    slopes(2, pieces)
+    slopes(3, pieces)
     relay(me)
-    fill = [functools.partial(slopes, p, pieces) for p in range(1, pieces)]
     count = len(arriving)
 
     def at(k):
         return arriving[k]
+
+    act_send = remote(
+        conv_act.at[pl.ds(0, tokens)], conv_act.at[pl.ds(tokens, tokens)], e_s.at[1], e_r.at[1], partner, t
+    )
 
     def normalize():
         for c in small:
@@ -280,137 +299,149 @@
         sigma = jax.nn.sigmoid(normed)
         dev_ref[...] = inverse
         hat_ref[...] = hat
-        conv_act[...] = (normed * sigma).astype(bf16)
+        conv_act[pl.ds(0, tokens), :] = (normed * sigma).astype(bf16)
+        act_send.start()
         slope_ref[...] = sigma * (1.0 + normed * (1.0 - sigma)) * gain_ref[...]
 
     outs = [r["gate_stage"], r["up_stage"], r["down_stage"], own_sum, r["value_stage"], r["grad_stage"]]
     stores = [pltpu.make_async_copy(d, r["result"][k], o_s.at[k]) for k, d in enumerate(outs)]
-    for i in range(count + 5):
-        if i - 5 >= 0 and i - 5 < count:
-            finish(at(i - 5), False)
-        if 0 <= i - 3 < count:
-            pair_up(at(i - 3))
-        if 0 <= i - 2 < count:
-            compute(at(i - 2), False)
-        if i < count:
-            arrive(at(i))
-            fan(at(i))
-        if i == 0:
-            relay(partner)
-        elif i - 1 < count:
-            relay(at(i - 1))
-        for _ in range(2 - i):
-            fill.pop(0)()
-        if i == min(3, count):
-            normalize()
-        if i == count:
-            compute(partner, False)
-            compute(me, False)
-        if i == count + 2:
-            pair_up(partner)
-            pair_up(me)
-            outs[2][...] = dots(act_ref[...], cot_rows[...], 0, 0).astype(bf16)
-            stores[2].start()
-        if i == count + 3:
-            outs[0][...] = dots(in_ref[...], delta[:, :hidden], 0, 0).astype(bf16)
-            stores[0].start()
-        if i == count + 4:
-            outs[1][...] = dots(in_ref[...], delta[:, hidden:], 0, 0).astype(bf16)
-            stores[1].start()
-    finish(partner, False)
-    finish(me, True)
-    for s in sp_peers:
-        from_home(s).wait_recv()
-    summed = dots(pick_any, home[...], 0, 0)
-    mix_full[:, lanes(t, width)] = (cot_ref[...].astype(f32) + summed).astype(bf16)
-
-    pieces = 2
-    piece_rows = tokens // pieces
-
-    def wide(k, column):
-        return mix_full.at[pl.ds(k * piece_rows, piece_rows), lanes(column, width)]
-
-    def wide_far(k):
-        return remote(wide(k, t), wide(k, t), wf_s.at[k], wf_r.at[k], me, far)
-
-    def wide_near(k):
-        return remote(wide(k, t), wide(k, t), wn_s.at[k], wn_r.at[k], me, near)
-
-    def wide_on(k):
-        return remote(wide(k, far), wide(k, far), wm_s.at[k], wm_r.at[k], me, near)
-
     pairs = group // 2
     parity = lax.rem(me, 2)
     half = me // 2
     ahead, behind = lax.rem(me + 1, group), lax.rem(me + group - 1, group)
-    alike = [lax.rem(half + o, pairs) for o in spread(pairs)]
-    order = alike + [half]
     columns = [t, near, far, cross]
-    sub = parts.shape[1]
-
-    def pair_swap(q, c):
-        side = lanes(columns[c], width)
-        return remote(
-            parts.at[2 * q + 1 - parity, :, side],
-            pair_in.at[q, :, side],
-            x_s.at[q, c],
-            x_r.at[q, c],
-            partner,
-            t,
-        )
-
-    def slot_of(source, target):
-        return lax.rem(target - source + pairs, pairs) - 1
-
-    def passing(source, target, c):
-        return others.at[slot_of(source, target), :, lanes(columns[c], width)], z_r.at[source, c]
-
-    def scatter(q, c):
-        slot, arrival = passing(half, q, c)
-        source = pair_sum.at[q, :, lanes(columns[c], width)]
-        return remote(source, slot, z_s.at[q, c], arrival, 2 * q + parity, t)
-
-    def project(c):
-        side = lanes(columns[c], width)
-        product = dots(conv_act[...], mix_full[:, side], 0, 0)
-        parts[:, :, side] = product.reshape(group, sub, width).astype(bf16)
-        for q in order:
-            pair_swap(q, c).start()
-
-    def absorb(q, c, own):
-        side = lanes(columns[c], width)
-        pair_swap(q, c).wait_recv()
-        both = parts[2 * q + parity, :, side].astype(f32) + pair_in[q, :, side].astype(f32)
-        if own:
-            own_sum[:, side] = both
+    sub = product.shape[1]
+    levels = pairs.bit_length() - 1
+    bits = [lax.rem(half // 2**j, 2) for j in range(levels)]
+    halo = beyond.shape[0]
+
+    def mixed(b, column, h):
+        return mix_both.at[pl.ds(b * tokens, tokens), piece_of(column, h)]
+
+    def wide_x(h):
+        return remote(mixed(0, t, h), mixed(1, t, h), x_s.at[h], x_r.at[h], partner, t)
+
+    def wide_far(b, h):
+        return remote(mixed(b, t, h), mixed(b, t, h), wf_s.at[b, h], wf_r.at[b, h], me, far)
+
+    def wide_near(b, h):
+        return remote(mixed(b, t, h), mixed(b, t, h), wn_s.at[b, h], wn_r.at[b, h], me, near)
+
+    def wide_on(b, h):
+        return remote(mixed(b, far, h), mixed(b, far, h), wm_s.at[b, h], wm_r.at[b, h], me, near)
+
+    def begin(h):
+        for s in sp_peers:
+            from_home(s, h).wait_recv()
+        side = pl.ds(h * hw, hw)
+        summed = dots(pick_any, home[:, side], 0, 0)
+        mix_both[pl.ds(0, tokens), piece_of(t, h)] = (cot_ref[:, side].astype(f32) + summed).astype(bf16)
+        wide_x(h).start()
+        wide_far(0, h).start()
+        wide_near(0, h).start()
+
+    def share(h):
+        wide_x(h).wait_recv()
+        wide_far(1, h).start()
+        wide_near(1, h).start()
+
+    def pass_on(b, h):
+        wide_far(b, h).wait_recv()
+        wide_on(b, h).start()
+
+    def gathered(kind, b, h):
+        if kind == 1:
+            spot_of, send, recv = mixed(b, near, h), wn_s, wn_r
         else:
-            pair_sum[q, :, side] = both.astype(bf16)
-            scatter(q, c).start()
-
-    tasks = [functools.partial(absorb, q, c, k == pairs - 1) for c in range(narrow) for k, q in enumerate(order)]
-
-    def run(number):
-        for _ in range(min(number, len(tasks))):
-            tasks.pop(0)()
-
-    for k in range(pieces):
-        wide_far(k).start()
-    for k in range(pieces):
-        wide_near(k).start()
-    project(0)
-    for k in range(pieces):
-        wide_near(k).wait_recv()
-    project(1)
-    for k in range(pieces):
-        wide_far(k).wait_recv()
-        wide_on(k).start()
-    run(pairs // 2)
+            spot_of, send, recv = mixed(b, cross, h), wm_s, wm_r
+        remote(spot_of, spot_of, send.at[b, h], recv.at[b, h], me, near).wait_recv()
+
+    def trade(g, j):
+        peer = 2 * (half + (1 - 2 * bits[j]) * 2**j) + parity
+        return remote(r["go%d" % j].at[g], r["come%d" % j].at[g], y_s.at[g, j], y_r.at[g, j], peer, t)
+
+    def project(c, h):
+        g = 2 * c + h
+        value = dots(conv_act[...], mix_both[:, piece_of(columns[c], h)], 0, 0)
+        product[...] = value.reshape(group, sub, hw)
+        for k in range(pairs // 2):
+            r["go0"][g, k] = product[2 * (2 * k + 1 - bits[0]) + parity].astype(bf16)
+            kept[g, k] = product[2 * (2 * k + bits[0]) + parity]
+        trade(g, 0).start()
+
+    def fold(c, h, j):
+        g = 2 * c + h
+        trade(g, j - 1).wait_recv()
+        left = pairs >> j
+        for k in range(left):
+            kept[g, k] = kept[g, k] + r["come%d" % (j - 1)][g, k].astype(f32)
+        if j < levels:
+            for k in range(left // 2):
+                r["go%d" % j][g, k] = kept[g, 2 * k + 1 - bits[j]].astype(bf16)
+            for k in range(left // 2):
+                kept[g, k] = kept[g, 2 * k + bits[j]]
+            trade(g, j).start()
+        else:
+            own_sum[:, piece_of(columns[c], h)] = kept[g, 0]
+
+    later = [functools.partial(pair_up, s, 1) for s in [me, partner] + arriving]
+    blocks = [me, partner] + arriving
+    for i in range(2, group + 4):
+        if i < group:
+            arrive(blocks[i])
+            fan(blocks[i])
+        if i - 1 < group:
+            relay(blocks[i - 1])
+        if i == min(5, group):
+            normalize()
+        if i - 2 < group:
+            compute(blocks[i - 2], False)
+        if 0 <= i - 3 < group:
+            pair_up(blocks[i - 3], 0)
+        if 0 <= i - 5 < group:
+            finish(blocks[i - 5], 0, i == 5)
+        if i > group:
+            for _ in range(len(later) // (group + 4 - i)):
+                later.pop(0)()
+    finish(blocks[group - 1], 0, False)
+    ending = [functools.partial(finish, s, 1, s is me) for s in blocks]
+    for f in ending[: group // 2]:
+        f()
+    outs[2][...] = dots(act_ref[...], cot_rows[...], 0, 0).astype(bf16)
+    stores[2].start()
+    begin(0)
+    for f in ending[group // 2 :]:
+        f()
+    outs[0][...] = dots(in_ref[...], delta[:, :hidden], 0, 0).astype(bf16)
+    stores[0].start()
+    share(0)
+    act_send.wait_recv()
+    project(0, 0)
+    pass_on(0, 0)
+    gathered(1, 0, 0)
+    gathered(1, 1, 0)
+    project(1, 0)
+    begin(1)
+    pass_on(1, 0)
+    project(2, 0)
+    gathered(2, 0, 0)
+    gathered(2, 1, 0)
+    project(3, 0)
+    outs[1][...] = dots(in_ref[...], delta[:, hidden:], 0, 0).astype(bf16)
+    stores[1].start()
+    fold(0, 0, 1)
+    fold(1, 0, 1)
+    share(1)
+    project(0, 1)
+    pass_on(0, 1)
+    gathered(1, 0, 1)
+    gathered(1, 1, 1)
+    project(1, 1)
+    fold(2, 0, 1)
+    fold(3, 0, 1)
     loads[9].wait()
-    project(2)
-    run(pairs // 2)
-    for k in range(pieces):
-        wide_on(k).wait_recv()
-    ng = dots(mix_full[...], w_ref[...], 1, 1) * slope_ref[...]
+    gathered(2, 0, 1)
+    ng = dots(mix_both[pl.ds(0, tokens), :], w_ref[...], 1, 1) * slope_ref[...]
     hat = hat_ref[...]
     sums = jnp.where(lane == 0, jnp.sum(ng, axis=1, keepdims=True), 0.0)
     sums = jnp.where(lane == 1, jnp.sum(ng * hat, axis=1, keepdims=True), sums)
@@ -419,7 +450,11 @@
     for k, p in enumerate((near, far, cross)):
         terms.append(remote(term_ref, terms_ref.at[k], u_s.at[k], u_r.at[k], me, p))
         terms[k].start()
-    run(pairs // 2)
+    pass_on(1, 1)
+    project(2, 1)
+    fold(0, 1, 1)
+    gathered(2, 1, 1)
+    project(3, 1)
     total = term_ref[...]
     for k, c in enumerate(terms):
         c.wait_recv()
@@ -427,10 +462,8 @@
     total = jnp.transpose(total)
     first, second = total[:, 0:1] / channels, total[:, 1:2] / channels
     extended[pl.ds(0, tokens), :] = dev_ref[...] * (ng - first - hat * second)
-    halo = beyond.shape[0]
     halo_send = remote(extended.at[pl.ds(0, halo)], beyond, e_s.at[0], e_r.at[0], behind, t)
     halo_send.start()
-    project(3)
     for c in loads[10:]:
         c.wait()
 
@@ -455,50 +488,50 @@
         return carry
 
     turns = (tokens // step - 1) * strips
-    rest = len(tasks) - 2
-    marks = [turns * i // rest for i in range(rest + 1)]
-    for i in range(rest):
-        run(1)
-        lax.fori_loop(marks[i], marks[i + 1], convolve, 0)
-    run(1)
-    halo_send.wait_recv()
-    tail_rows = beyond[...]
-    extended[pl.ds(tokens, halo), :] = jnp.where(me == group - 1, jnp.zeros_like(tail_rows), tail_rows)
-    lax.fori_loop(turns, turns + strips, convolve, 0)
-    stores[4].start()
-    stores[5].start()
-    run(1)
-    for c in range(narrow):
-        side = lanes(columns[c], width)
-        total = own_sum[:, side]
-        for q in alike:
-            slot, arrival = passing(q, half, c)
-            remote(pair_sum.at[q, :, side], slot, z_s.at[q, c], arrival, 2 * q + parity, t).wait_recv()
-            total = total + others[slot_of(q, half), :, side].astype(f32)
-        own_sum[:, side] = total
+    line = [(0, 0), (1, 0), (2, 0), (3, 0), (0, 1), (1, 1), (2, 1), (3, 1)]
+    tasks = [(*g, 1) for g in line[5:]]
+    for j in range(2, levels + 1):
+        tasks += [(*g, j) for g in line]
+    tasks.sort(key=lambda x: line.index(x[:2]) + 3 * x[2])
+    cuts = len(tasks) - 2
+    marks = [turns * i // cuts for i in range(cuts + 1)]
+    for i, task in enumerate(tasks):
+        if i == cuts:
+            halo_send.wait_recv()
+            tail_rows = beyond[...]
+            extended[pl.ds(tokens, halo), :] = jnp.where(me == group - 1, jnp.zeros_like(tail_rows), tail_rows)
+            lax.fori_loop(turns, turns + strips, convolve, 0)
+            stores[4].start()
+            stores[5].start()
+        fold(*task)
+        if i < cuts:
+            lax.fori_loop(marks[i], marks[i + 1], convolve, 0)
     stores[3].start()
     for s in [me] + sp_peers:
         to_far(s).wait_send()
         to_near(s).wait_send()
         onward(s).wait_send()
-        part_near(s, 0).wait_send()
-        part_near(s, 1).wait_send()
-        part_far(s).wait_send()
+        for h in range(2):
+            part_near(s, 0, h).wait_send()
+            part_near(s, 1, h).wait_send()
+            part_far(s, h).wait_send()
     for s in sp_peers:
         swap(s).wait_send()
-        to_home(s).wait_send()
+        to_home(s, 0).wait_send()
+        to_home(s, 1).wait_send()
     for c in small + terms:
         c.wait_send()
-    for k in range(pieces):
-        wide_far(k).wait_send()
-        wide_near(k).wait_send()
-        wide_on(k).wait_send()
+    for h in range(2):
+        wide_x(h).wait_send()
+        for b in range(2):
+            wide_far(b, h).wait_send()
+            wide_near(b, h).wait_send()
+            wide_on(b, h).wait_send()
     halo_send.wait_send()
-    for c in range(narrow):
-        for q in order:
-            pair_swap(q, c).wait_send()
-        for q in alike:
-            scatter(q, c).wait_send()
+    act_send.wait_send()
+    for g in range(2 * narrow):
+        for j in range(levels):
+            trade(g, j).wait_send()
     for c in stores:
         c.wait()
 
@@ -533,6 +566,8 @@
         gain=VMEM(gain.shape, f32),
         pair_w=VMEM((model, 2 * hidden), bf16),
         down=VMEM(down_w.shape, bf16),
+        down_t=VMEM((model, hidden), bf16),
+        pair_t=VMEM((2 * hidden, model), bf16),
         proj=VMEM(proj_w.shape, bf16),
         taps=VMEM(taps.shape, f32),
         value=VMEM(tile, bf16),
@@ -553,15 +588,13 @@
         stats=VMEM((narrow, 8, tokens), f32),
         term=VMEM((8, tokens), f32),
         terms=VMEM((narrow - 1, 8, tokens), f32),
-        mix_full=VMEM((tokens, model), bf16),
-        parts=VMEM((group, sub, model), bf16),
-        pair_in=VMEM((pairs, sub, model), bf16),
-        pair_sum=VMEM((pairs, sub, model), bf16),
-        others=VMEM((pairs - 1, sub, model), bf16),
+        mix_both=VMEM((2 * tokens, model), bf16),
+        product=VMEM((group, sub, width // 2), f32),
+        kept=VMEM((2 * narrow, pairs // 2, sub, width // 2), f32),
         own_sum=VMEM((sub, model), f32),
         extended=VMEM((tokens + halo, width), f32),
         beyond=VMEM((halo, width), f32),
-        conv_act=VMEM(tile, bf16),
+        conv_act=VMEM((2 * tokens, width), bf16),
         hat=VMEM(tile, f32),
         slope=VMEM(tile, f32),
         dev=VMEM((tokens, 1), f32),
@@ -572,19 +605,25 @@
         grad_stage=VMEM(tile, bf16),
         l_s=dma((len(args),)),
         o_s=dma((len(results),)),
-        e_s=dma((1,)),
-        e_r=dma((1,)),
+        e_s=dma((2,)),
+        e_r=dma((2,)),
     )
     scratch["in"] = VMEM(rows_in.shape, bf16)
-    for n in ("a", "n", "f", "m", "pf", "h"):
+    levels = pairs.bit_length() - 1
+    for j in range(levels):
+        held = VMEM((2 * narrow, pairs >> (j + 1), sub, width // 2), bf16)
+        scratch["go%d" % j] = scratch["come%d" % j] = held
+    for n in ("a", "n", "f", "m"):
         scratch[n + "_s"] = scratch[n + "_r"] = dma((group,))
-    scratch["pn_s"] = scratch["pn_r"] = dma((group, 2))
+    for n in ("pf", "h"):
+        scratch[n + "_s"] = scratch[n + "_r"] = dma((group, 2))
+    scratch["pn_s"] = scratch["pn_r"] = dma((group, 4))
     for n in ("t", "u"):
         scratch[n + "_s"] = scratch[n + "_r"] = dma((narrow - 1,))
     for n in ("wn", "wf", "wm"):
-        scratch[n + "_s"] = scratch[n + "_r"] = dma((2,))
-    for n in ("x", "z"):
-        scratch[n + "_s"] = scratch[n + "_r"] = dma((pairs, narrow))
+        scratch[n + "_s"] = scratch[n + "_r"] = dma((2, 2))
+    scratch["x_s"] = scratch["x_r"] = dma((2,))
+    scratch["y_s"] = scratch["y_r"] = dma((2 * narrow, levels))
 
     def body(*refs):
         whole_kernel(group, narrow, cap, len(args), len(results), tuple(scratch), *refs)

time: 93.7 us -> 84.3 us (0.90)
  Pallas kernels: 92.5 us -> 83.3 us
    pallas_call x1, Pallas kernels: 90.4 us -> 81.3 us  [whole_pass(): pl.pallas_call(body, name='whole_kernel', out_shape=tuple((jax.ShapeDtype...]
where the time goes in v4:
time: 84.3 us; the launch traced here: 84.1 us
  Pallas kernels  83.3 us (99%)
    pallas_call x1, Pallas kernels, whole_pass(): pl.pallas_call(body, name='whole_kernel', out_shape=tuple((jax.ShapeDtype...  81.3 us
    pallas_call x1, Pallas kernels, emit(): pl.pallas_call(functools.partial(emit_kernel, len(results)), name='emit',...  2.05 us

profile of v4, /device:TPU:0, one launch (start us, length us, event | category | flops | bytes accessed | tf_op | source)
XLA Modules:
  0.0 84.1 jit_solution(3342945597956898452)
XLA Ops:
  0.6 81.3 %whole_kernel.1 = (bf16[2048,256]{1,0:T(8,128)(2,1)S(1)}, bf16[2048,256]{1,0:T(8,128)(2,1)S(1)}, bf16[256,2048]{1,0:T(8,128)(2,1)S(1)}, f32[64,2048]{1,0:T(8,128...) custom-call(s32[2,256]{1,0:T(2,128)} %bitcast.14, f32[2,256]{1,0:T(2,128)} %bitcast.15, ...), custom_call_target="tpu_custom_call" | custom-call | tf_op jit(solution)/shard_map/whole_kernel/pallas_call | solution.py:631
  81.9 2.1 %emit.1 = (bf16[2048,256]{1,0:T(8,128)(2,1)}, bf16[2048,256]{1,0:T(8,128)(2,1)}, bf16[256,2048]{1,0:T(8,128)(2,1)}, f32[64,2048]{1,0:T(8,128)}, bf16[256,512]{1,0:T(8,128)(2,1)}, /*index=5*/bf16[256,512]{1,0:T(8,128)(2,1)}) custom-call(bf16[2048,256]{1,0:T(8,128)(2,1)S(1)} %get-tuple-element.18.refs_0_, bf16[2048,256]{1,0:T(8,128)(2,1)S(1)} %get-tuple-element.19.refs_1_, ...), custom_call_target="tpu_custom_call" | custom-call | tf_op jit(solution)/shard_map/emit/pallas_call | solution.py:654
